TPU v7x, 512 devices: a whole 4x4x16 slice. The times are simulated.
512 devices in a mesh: ep: 16 (over y, x), tp: 32 (over z, core).
Axes of the slice: x: 4, y: 4, z: 16, core: 2. Of those that a mesh axis runs over, the one named last changes fastest.
Arguments:
- tokens: bfloat16 [512, 2048], P('ep'), may hold values from -6 to 6
- norm_gain: float32 [2048], replicated, may hold values from 0.1 to 1.9
- routes: int32 [512, 2], P('ep'), may hold values from 0 to 15, all different within a row; in each aligned block of 32 rows (0 to 31, 32 to 63, ...) at most 16 rows name the same one
- gate_weights: float32 [512, 2], P('ep'), may hold values from 0.1 to 1
- expert_gate: bfloat16 [16, 2048, 8192], P('ep', None, 'tp'), may hold values from -0.125 to 0.125
- expert_up: bfloat16 [16, 2048, 8192], P('ep', None, 'tp'), may hold values from -0.125 to 0.125
- expert_down: bfloat16 [16, 8192, 2048], P('ep', 'tp'), may hold values from -0.0625 to 0.0625
Outputs:
- mixed: bfloat16 [512, 2048], P('ep', 'tp')
Inputs may be any that keep to these rules, and one draw needn't show every extreme that they name: `routes`: each row names 2 different experts; among the rows of one index of ep no expert is named by more than 16 rows.
All inputs are finite; a program needn't handle non-finite values.
Results may differ from a plain program's by a relative error of at most 0.0095.
Values may be sent and summed in bfloat16 or wider, within the bound.
No kernel may reach another device: no remote copies, remote signals or barrier semaphores. Data moves between devices by JAX's collectives and lax.ppermute only.
A program may use at most 64 MiB of HBM per device.

v0:
```python
import jax
import jax.numpy as jnp
from jax import lax
from jax.sharding import PartitionSpec as P


def in_blocks(x, dim, peers):
    before, after = (x.shape[:dim], x.shape[dim + 1 :])
    return jnp.moveaxis(x.reshape(*before, peers, -1, *after), dim, 0)


def summed_on_arrival(x, axis, dim):
    blocks = in_blocks(x, dim, lax.axis_size(axis))
    arrived = lax.all_to_all(blocks, axis, split_axis=0, concat_axis=0, tiled=True)
    return arrived.astype(jnp.float32).sum(axis=0)


def expert_rows(rows, w_gate, w_up):
    gate = jnp.dot(rows, w_gate, preferred_element_type=jnp.float32)
    upper = jnp.dot(rows, w_up, preferred_element_type=jnp.float32)
    return (jax.nn.silu(gate) * upper).astype(jnp.bfloat16)


def shards(tokens, norm_gain, routes, gate_weights, expert_gate, expert_up, expert_down):
    tok_rows, width = tokens.shape
    n_ep = lax.axis_size("ep")
    n_tp = lax.axis_size("tp")
    part_width = width // n_tp
    values = tokens.astype(jnp.float32)
    scale = lax.rsqrt(jnp.mean(values * values, axis=-1, keepdims=True) + 1e-06)
    normed = (values * scale * norm_gain[None, :]).astype(jnp.bfloat16)
    w_gate = expert_gate[0]
    w_up = expert_up[0]
    w_down = expert_down[0]
    capacity = tok_rows // 2
    picks = routes.reshape(-1)
    chosen = (picks[:, None] == jnp.arange(n_ep, dtype=jnp.int32)[None, :]).astype(jnp.int32)
    ranks = jnp.cumsum(chosen, axis=0) - chosen
    place = picks * capacity + jnp.sum(ranks * chosen, axis=1)
    table = (place[None, :] == jnp.arange(n_ep * capacity, dtype=jnp.int32)[:, None]).astype(
        jnp.float32
    )
    slots = jnp.sum(table.reshape(n_ep * capacity, tok_rows, 2), axis=2)
    buffer = jnp.dot(slots.astype(jnp.bfloat16), normed, preferred_element_type=jnp.float32)
    buffer = buffer.astype(jnp.bfloat16).reshape(n_ep, capacity, width)
    combine = jnp.sum(
        (table * gate_weights.reshape(-1)[None, :]).reshape(n_ep * capacity, tok_rows, 2), axis=2
    ).T
    received = lax.all_to_all(buffer, "ep", split_axis=0, concat_axis=0, tiled=True)
    sources = received.shape[0]
    count = received.shape[1]
    hidden = expert_rows(received.reshape(sources * count, width), w_gate, w_up)
    partial_value = jnp.dot(hidden, w_down, preferred_element_type=jnp.float32)
    outputs = summed_on_arrival(
        partial_value.reshape(sources, count, width).astype(jnp.bfloat16), "tp", 2
    )
    back = lax.all_to_all(outputs, "ep", split_axis=0, concat_axis=0, tiled=True)
    mixed = jnp.dot(
        combine,
        back.reshape(n_ep * capacity, part_width),
        precision=lax.Precision.HIGHEST,
        preferred_element_type=jnp.float32,
    )
    return mixed.astype(jnp.bfloat16)


def solution(mesh):
    placed = (
        P("ep", None),
        P(),
        P("ep", None),
        P("ep", None),
        P("ep", None, "tp"),
        P("ep", None, "tp"),
        P("ep", "tp", None),
    )
    return jax.shard_map(
        shards, mesh=mesh, in_specs=placed, out_specs=P("ep", "tp"), check_vma=False
    )
```

profile of v0, /device:TPU:1, one launch (start us, length us, event | category | flops | bytes accessed | tf_op | source)
XLA Modules:
  0.0 129.4 jit_solution(18074268864938607713)
XLA Ops:
  0.0 0.0 copy-start
  0.0 0.0 copy-start.1
  0.0 0.9 copy.26
  0.9 0.1 eq.30
  1.0 0.1 fusion.11
  1.1 0.1 reduce_window_sum.11
  1.2 0.2 select_reduce_fusion.1
  1.4 0.1 reduce_sum.48
  1.5 0.1 copy.27
  1.6 0.7 multiply_add_fusion
  2.3 1.0 fusion.5
  3.3 0.8 convert_reduce_fusion.1
  4.1 1.4 %convolution_convert_fusion.1 = bf16[256,2048]{1,0:T(8,128)(2,1)S(1)} fusion(bf16[32,2048]{1,0:T(8,128)(2,1)} %param.7, f32[2048]{0:T(1024)} %param.8, f32[32]{0:T(128)S(1)} %add_rsqrt_fusion, bf16[256,32]{0,1:T(8,128)(2,1)S(1)} %get-tuple-element.5), kind=kOutput, calls=%fused_computation.2 | convolution fusion | flops 34340864 | bytes 1204352 | tf_op jit(solution)/shard_map/dot_general | solution.py:44
  5.5 0.0 copy-start.2
  5.5 22.8 %all_to_all.15 = bf16[16,16,2048]{2,1,0:T(8,128)(2,1)S(1)} all-to-all(bf16[16,16,2048]{2,1,0:T(8,128)(2,1)S(1)} %bitcast.24), channel_id=1, replica_groups=mesh['ep'=16,'tp'=32] {'ep'}, dimensions={0} | all-to-all | bytes 2097152 | tf_op jit(solution)/shard_map/all_to_all | solution.py:49
  28.3 0.0 copy-done.1
  28.3 0.4 fusion.3
  28.8 0.0 copy-done.2
  28.8 0.4 fusion
  29.2 0.0 copy-done
  29.3 1.4 %convolution_convert_fusion = bf16[16,16,2048]{2,1,0:T(8,128)(2,1)} fusion(bf16[16,16,256]{2,1,0:T(8,128)(2,1)S(1)} %bitcast.28, bf16[1,256,2048]{2,1,0:T(8,128)(2,1)S(1)} %copy-done), kind=kOutput, calls=%fused_computation.1 | convolution fusion | flops 268959744 | bytes 2228224 | tf_op jit(solution)/shard_map/dot_general | solution.py:53
  30.7 3.3 %reshape.59 = bf16[16,16,32,64]{3,2,1,0:T(8,128)(2,1)S(1)} reshape(bf16[16,16,2048]{2,1,0:T(8,128)(2,1)} %convolution_convert_fusion) | data formatting | bytes 2097152 | tf_op jit(solution)/shard_map/reshape | solution.py:9
  34.0 2.2 %copy.30 = bf16[16,16,32,64]{3,1,0,2:T(8,128)(2,1)} copy(bf16[16,16,32,64]{3,2,1,0:T(8,128)(2,1)S(1)} %reshape.59) | data formatting | bytes 2097152 | tf_op jit(solution)/shard_map/reshape | solution.py:9
  36.2 3.9 %reshape.62 = bf16[32,2,8192]{2,1,0:T(2,128)(2,1)S(1)} reshape(bf16[32,16,16,64]{3,2,1,0:T(8,128)(2,1)} %bitcast.23) | data formatting | bytes 2097152
  40.1 73.6 %all_to_all.16 = bf16[32,2,8192]{2,1,0:T(2,128)(2,1)} all-to-all(bf16[32,2,8192]{2,1,0:T(2,128)(2,1)S(1)} %reshape.62), channel_id=1, replica_groups=mesh['ep'=16,'tp'=32] {'tp'}, dimensions={0} | all-to-all | bytes 2097152 | tf_op jit(solution)/shard_map/all_to_all | solution.py:14
  113.7 3.8 %reshape.63 = bf16[32,16,16,64]{3,2,1,0:T(8,128)(2,1)S(1)} reshape(bf16[32,2,8192]{2,1,0:T(2,128)(2,1)} %all_to_all.16) | data formatting | bytes 2097152
  117.4 0.4 convert_reduce_fusion
  117.9 0.1 reshape.64
  118.0 9.2 %all_to_all.17 = f32[16,1,1024]{2,1,0:T(1,128)S(1)} all-to-all(f32[16,1,1024]{2,1,0:T(1,128)S(1)} %reshape.64), channel_id=1, replica_groups=mesh['ep'=16,'tp'=32] {'ep'}, dimensions={0} | all-to-all | bytes 131072 | tf_op jit(solution)/shard_map/all_to_all | solution.py:57
  127.2 0.5 broadcast.42
  127.7 0.8 reduce
  128.5 0.1 reshape.65
  128.6 0.8 convolution_convert_fusion.2
  (1 shorter events, 0.0 us)
Async XLA Ops:
  0.0 29.2 %copy-start = (bf16[1,256,2048]{2,1,0:T(8,128)(2,1)S(1)}, bf16[1,256,2048]{2,1,0:T(8,128)(2,1)}, u32[]{:S(2)}) copy-start(bf16[1,256,2048]{2,1,0:T(8,128)(2,1)} %param.13) | copy-start | bytes 3145732
  0.0 28.3 %copy-start.1 = (bf16[1,2048,256]{2,1,0:T(8,128)(2,1)S(1)}, bf16[1,2048,256]{2,1,0:T(8,128)(2,1)}, u32[]{:S(2)}) copy-start(bf16[1,2048,256]{2,1,0:T(8,128)(2,1)} %param.11) | copy-start | bytes 3145732
  5.5 23.3 %copy-start.2 = (bf16[1,2048,256]{2,1,0:T(8,128)(2,1)S(1)}, bf16[1,2048,256]{2,1,0:T(8,128)(2,1)}, u32[]{:S(2)}) copy-start(bf16[1,2048,256]{2,1,0:T(8,128)(2,1)} %param.12) | copy-start | bytes 3145732
where the time goes:
time: 130 us; the launch traced here: 129 us
  blocking collectives  106 us (82%)
  local copies, waits for them, and re-layouts  15.1 us (12%)
  matrix products  4.49 us (3%)
  other arithmetic  4.08 us (3%)
    all_to_all x1, blocking collectives, summed_on_arrival(): lax.all_to_all(blocks, axis, split_axis=0, concat_axis=0, tiled=True)  73.6 us
    all_to_all x1, blocking collectives, shards(): lax.all_to_all(buffer, 'ep', split_axis=0, concat_axis=0, tiled=True)  22.8 us
    all_to_all x1, blocking collectives, shards(): lax.all_to_all(outputs, 'ep', split_axis=0, concat_axis=0, tiled=True)  9.2 us
    unnamed x11, local copies, waits for them, and re-layouts  8.79 us
    reshape x2, local copies, waits for them, and re-layouts, in_blocks(): return jnp.moveaxis(x.reshape(*before, peers, -1, *after), dim, 0)  5.49 us

commit v1 on v0

v1 whole, which is shorter than its diff:
```python
import jax
import jax.numpy as jnp
import numpy as np
from jax import lax
from jax.experimental import pallas as pl
from jax.experimental.pallas import tpu as pltpu
from jax.sharding import Mesh
from jax.sharding import PartitionSpec as P

LANES = 128
HALF = LANES // 2
F32 = jnp.float32
BF16 = jnp.bfloat16
SWAP = ((0, 1), (1, 0))


def params(mib):
    return pltpu.CompilerParams(vmem_limit_bytes=mib * 2**20)


def flipped(x):
    return pltpu.roll(x, HALF, axis=x.ndim - 1)


def column(row, eye):
    return jnp.sum(jnp.where(eye, row, 0), axis=1, keepdims=True)


def dispatch_kernel(tok_ref, gain_ref, picks_ref, weight_ref, buffer_ref, combine_ref):
    rows, width = tok_ref.shape
    slots = buffer_ref.shape[0]
    cap = rows // 2
    part = width // 2
    first = pl.multiple_of(lax.axis_index("c") * part, part)
    values = tok_ref[...].astype(F32)
    scale = lax.rsqrt(jnp.mean(values * values, axis=-1, keepdims=True) + 1e-06)
    mine = tok_ref[:, pl.ds(first, part)].astype(F32)
    normed = (mine * scale * gain_ref[:, pl.ds(first, part)]).astype(BF16)

    at_row = lax.broadcasted_iota(jnp.int32, (rows, rows), 0)
    at_col = lax.broadcasted_iota(jnp.int32, (rows, rows), 1)
    eye = at_row == at_col
    earlier = (at_col < at_row).astype(F32).astype(BF16)
    pick0 = column(picks_ref[0:1, :], eye)
    pick1 = column(picks_ref[1:2, :], eye)
    weight0 = column(weight_ref[0:1, :], eye)
    weight1 = column(weight_ref[1:2, :], eye)
    slot = lax.broadcasted_iota(jnp.int32, (rows, slots), 1)
    expert = slot // cap
    place = (slot % cap).astype(F32)
    is0 = pick0 == expert
    is1 = pick1 == expert
    chosen = (is0 | is1).astype(F32)
    rank = jnp.dot(earlier, chosen.astype(BF16), preferred_element_type=F32)
    table = jnp.where(rank == place, chosen, 0.0)
    buffer_ref[...] = jnp.dot(
        table.T.astype(BF16), normed, preferred_element_type=F32
    ).astype(BF16)
    weights = table * jnp.where(is0, weight0, weight1)
    high = weights.astype(BF16)
    combine_ref[0:rows, :] = high
    combine_ref[rows:, :] = (weights - high.astype(F32)).astype(BF16)


def first_half_kernel(rows_ref, gate_ref, up_ref, gate_out, up_out):
    part = rows_ref.shape[1]
    first = pl.multiple_of(lax.axis_index("c") * part, part)
    rows = rows_ref[...]
    gate_out[...] = jnp.dot(rows, gate_ref[pl.ds(first, part), :], preferred_element_type=F32)
    up_out[...] = jnp.dot(rows, up_ref[pl.ds(first, part), :], preferred_element_type=F32)


def expert_kernel(rows_ref, gate_in, up_in, gate_ref, up_ref, down_ref, mine_out, send_out):
    part = rows_ref.shape[1]
    core = lax.axis_index("c")
    first = pl.multiple_of((1 - core) * part, part)
    rows = rows_ref[...]
    gate = gate_in[...] + jnp.dot(
        rows, gate_ref[pl.ds(first, part), :], preferred_element_type=F32
    )
    upper = up_in[...] + jnp.dot(rows, up_ref[pl.ds(first, part), :], preferred_element_type=F32)
    hidden = (gate / (1.0 + jnp.exp(-gate)) * upper).astype(BF16)
    is_low = core == 0
    lane = lax.broadcasted_iota(jnp.int32, (rows.shape[0], LANES), 1)
    low_lane = lane < HALF
    stay = low_lane == is_low
    for m in range(mine_out.shape[1] // LANES):
        pair = jnp.dot(
            hidden, down_ref[:, 2 * m * LANES : 2 * (m + 1) * LANES], preferred_element_type=F32
        )
        a, b = pair[:, :LANES], pair[:, LANES:]
        at = slice(m * LANES, (m + 1) * LANES)
        keep, move = jnp.where(is_low, a, b), jnp.where(is_low, b, a)
        mine_out[:, at] = jnp.where(stay, keep, flipped(move))
        send_out[:, at] = jnp.where(stay, flipped(keep), move).astype(BF16)


def combine_kernel(table_ref, back_ref, out_ref):
    rows = table_ref.shape[0] // 2
    half = rows // 2
    both = jnp.dot(table_ref[...], back_ref[...], preferred_element_type=F32)
    mixed = both[:rows] + both[rows:]
    low_lane = lax.broadcasted_iota(jnp.int32, (half, LANES), 1) < HALF
    for m in range(back_ref.shape[1] // LANES):
        at = slice(m * LANES, (m + 1) * LANES)
        a, b = mixed[:half, at], mixed[half:, at]
        out_ref[2 * m] = jnp.where(low_lane, a, flipped(b)).astype(BF16)
        out_ref[2 * m + 1] = jnp.where(low_lane, flipped(a), b).astype(BF16)


def total_kernel(parts_ref, out_ref):
    half = out_ref.shape[0] // 2
    total = jnp.sum(parts_ref[...].astype(F32), axis=0)
    out_ref[:half, :] = total[:, :HALF].astype(BF16)
    out_ref[half:, :] = flipped(total)[:, :HALF].astype(BF16)


def shape(dims, dtype):
    return jax.ShapeDtypeStruct(dims, dtype)


def shards(tokens, norm_gain, routes, gate_weights, expert_gate, expert_up, expert_down):
    rows, width = tokens.shape
    n_ep = lax.axis_size("ep")
    n_z = lax.axis_size("z")
    cap = rows // 2
    slots = n_ep * cap
    part = width // 2
    w_gate, w_up, w_down = expert_gate[0], expert_up[0], expert_down[0]
    units = w_gate.shape[1]

    buffer, table = pl.pallas_call(
        dispatch_kernel,
        out_shape=(shape((slots, part), BF16), shape((2 * rows, slots), BF16)),
        compiler_params=params(8),
        name="dispatch",
    )(tokens, norm_gain[None, :], routes.T, gate_weights.T)
    received = lax.all_to_all(
        buffer.reshape(n_ep, cap, part), "ep", split_axis=0, concat_axis=0, tiled=True
    ).reshape(slots, part)
    other = lax.ppermute(received, "c", SWAP)
    gate, upper = pl.pallas_call(
        first_half_kernel,
        out_shape=(shape((slots, units), F32), shape((slots, units), F32)),
        compiler_params=params(8),
        name="first_half",
    )(received, w_gate, w_up)
    mine, send = pl.pallas_call(
        expert_kernel,
        out_shape=(shape((slots, part), F32), shape((slots, part), BF16)),
        compiler_params=params(12),
        name="expert",
    )(other, gate, upper, w_gate, w_up, w_down)
    arrived = lax.ppermute(send, "c", SWAP)
    outputs = (mine + arrived.astype(F32)).astype(BF16)
    back = lax.all_to_all(
        outputs.reshape(n_ep, cap, part), "ep", split_axis=0, concat_axis=0, tiled=True
    ).reshape(slots, part)
    packed = pl.pallas_call(
        combine_kernel,
        out_shape=shape((n_z, rows // 2, LANES), BF16),
        compiler_params=params(8),
        name="combine",
    )(table, back)
    parts = lax.all_to_all(packed, "z", split_axis=0, concat_axis=0, tiled=True)
    return pl.pallas_call(
        total_kernel,
        out_shape=shape((rows, HALF), BF16),
        compiler_params=params(8),
        name="total",
    )(parts)


def solution(mesh):
    n_ep, n_tp = mesh.devices.shape
    chips = Mesh(np.asarray(mesh.devices).reshape(n_ep, n_tp // 2, 2), ("ep", "z", "c"))
    tp = ("z", "c")
    placed = (
        P("ep", None),
        P(),
        P("ep", None),
        P("ep", None),
        P("ep", None, tp),
        P("ep", None, tp),
        P("ep", tp, None),
    )
    return jax.shard_map(
        shards, mesh=chips, in_specs=placed, out_specs=P("ep", tp), check_vma=False
    )
```

time: 130 us -> 75.2 us (0.58)
  blocking collectives: 106 us -> 56.8 us
  local copies, waits for them, and re-layouts: 15.1 us -> 5.36 us
  starting transfers between devices: 0 us -> 6.74 us
  matrix products: 4.49 us -> 0 us
  other arithmetic: 4.08 us -> 0.14 us
  Pallas kernels: 0 us -> 2.99 us
  waiting for transfers between devices: 0 us -> 1.88 us
    all_to_all x3, blocking collectives: 106 us -> 56.8 us  [the longest x1 26.3 us: shards(): parts = lax.all_to_all(packed, 'z', split_axis=0, concat_axis=0, tiled=True)]
    ppermute x0 -> x2, starting transfers between devices: none -> 6.74 us  [the longest x1 4.81 us: shards(): other = lax.ppermute(received, 'c', SWAP)]
    reshape x2 -> x0, local copies, waits for them, and re-layouts: 5.49 us -> none  [in_blocks(): return jnp.moveaxis(x.reshape(*before, peers, -1, *after), dim, 0)]
    dot_general x5 -> x0, matrix products: 4.49 us -> none  [the longest x1 1.43 us: shards(): partial_value = jnp.dot(hidden, w_down, preferred_element_type=jnp.float32)]
    unnamed x11 -> x16, local copies, waits for them, and re-layouts: 8.79 us -> 5.36 us
    pallas_call x0 -> x5, Pallas kernels: none -> 2.99 us  [the longest x1 1.03 us: shards(): pl.pallas_call(expert_kernel, out_shape=(shape((slots, part), F32), shape...]
    reduce_sum x4 -> x0, other arithmetic: 2.41 us -> none  [the longest x1 1.04 us: shards(): scale = lax.rsqrt(jnp.mean(values * values, axis=-1, keepdims=True) + 1e-06)]
    ppermute x0 -> x2, waiting for transfers between devices: none -> 1.88 us  [the longest x1 1.87 us: shards(): arrived = lax.ppermute(send, 'c', SWAP)]
  transfers between devices with their start and end apart: 0 -> 2, of which waited for: 0 -> 1; matrix products, arithmetic and copies ran while one was open for 0% -> 0% of each run, Pallas kernels for 0% -> 1%
where the time goes in v1:
time: 75.2 us; the launch traced here: 74 us
  blocking collectives  56.8 us (76%)
  starting transfers between devices  6.74 us (9%)
  local copies, waits for them, and re-layouts  5.36 us (7%)
  Pallas kernels  2.99 us (4%)
  waiting for transfers between devices  1.88 us (2%)
    all_to_all x1, blocking collectives, shards(): parts = lax.all_to_all(packed, 'z', split_axis=0, concat_axis=0, tiled=True)  26.3 us
    all_to_all x1, blocking collectives, shards(): lax.all_to_all(buffer.reshape(n_ep, cap, part), 'ep', split_axis=0, conca...  17 us
    all_to_all x1, blocking collectives, shards(): lax.all_to_all(outputs.reshape(n_ep, cap, part), 'ep', split_axis=0, conc...  13.5 us
    unnamed x16, local copies, waits for them, and re-layouts  5.36 us
    ppermute x1, starting transfers between devices, shards(): other = lax.ppermute(received, 'c', SWAP)  4.81 us
    ppermute x1, starting transfers between devices, shards(): arrived = lax.ppermute(send, 'c', SWAP)  1.92 us
    ppermute x1, waiting for transfers between devices, shards(): arrived = lax.ppermute(send, 'c', SWAP)  1.87 us
  transfers between devices with their start and end apart: 2, of which 1 were waited for; matrix products, arithmetic and copies ran while one was open for 0% of the time, Pallas kernels for 1%

profile of v1, /device:TPU:1, one launch (start us, length us, event | category | flops | bytes accessed | tf_op | source)
XLA Modules:
  0.0 74.0 jit_solution(13428187737402979757)
XLA Ops:
  0.0 0.0 copy-start
  0.0 0.0 copy-start.4
  0.0 1.0 %copy-done.4 = bf16[32,2048]{1,0:T(8,128)(2,1)S(1)} copy-done((bf16[32,2048]{1,0:T(8,128)(2,1)S(1)}, bf16[32,2048]{1,0:T(8,128)(2,1)}, u32[]{:S(2)}) %copy-start.4) | copy-done | bytes 131096
  1.0 0.0 copy-start.5
  1.0 0.7 copy-done.5
  1.7 0.0 copy-start.6
  1.7 0.7 copy-done.6
  2.4 0.0 copy-start.7
  2.4 0.7 copy-done.7
  3.1 0.6 dispatch.1
  3.6 17.0 %all_to_all.15 = bf16[16,16,1024]{2,1,0:T(8,128)(2,1)S(1)} all-to-all(bf16[16,16,1024]{2,1,0:T(8,128)(2,1)S(1)} %bitcast.18), channel_id=1, replica_groups=mesh['ep'=16,'z'=16,'c'=2] {'ep'}, dimensions={0} | all-to-all | bytes 1048576 | tf_op jit(solution)/shard_map/all_to_all | solution.py:138
  20.6 4.8 %collective-permute-start = (bf16[256,1024]{1,0:T(8,128)(2,1)S(1)}, bf16[256,1024]{1,0:T(8,128)(2,1)S(1)}, u32[]{:S(2)}, u32[]{:S(2)}) collective-permute-start(bf16[256,1024]{1,0:T(8,128)(2,1)S(1)} %bitcast.14), channel_id=1, source_target_pairs={{0,1},{1,0},{2,3},{3,2},{4,5},{5,4},{6,7},{7,6},{8,9},{9,8},{10,11... | collective-permute-start | bytes 1572872 | tf_op jit(solution)/shard_map/ppermute | solution.py:141
  25.4 0.0 copy-done
  25.4 0.0 copy-start.1
  25.4 1.2 %copy-done.1 = bf16[1,2048,256]{2,1,0:T(8,128)(2,1)S(1)} copy-done((bf16[1,2048,256]{2,1,0:T(8,128)(2,1)S(1)}, bf16[1,2048,256]{2,1,0:T(8,128)(2,1)}, u32[]{:S(2)}) %copy-start.1) | copy-done | bytes 1048600
  26.7 0.0 copy-start.2
  26.7 0.0 copy-start.3
  26.7 0.4 first_half.1
  27.1 0.0 collective-permute-done.rows_ref
  27.1 0.8 %copy-done.2 = bf16[1,2048,256]{2,1,0:T(8,128)(2,1)S(1)} copy-done((bf16[1,2048,256]{2,1,0:T(8,128)(2,1)S(1)}, bf16[1,2048,256]{2,1,0:T(8,128)(2,1)}, u32[]{:S(2)}) %copy-start.2) | copy-done | bytes 1048600
  27.9 0.3 copy-done.3
  28.2 1.0 %expert.1 = (f32[256,1024]{1,0:T(8,128)S(1)}, bf16[256,1024]{1,0:T(8,128)(2,1)S(1)}) custom-call(bf16[256,1024]{1,0:T(8,128)(2,1)S(1)} %collective-permute-done.rows_ref, f32[256,256]{1,0:T(8,128)S(1)} %get-tuple-element.13.gate_in, f32[256,256]{1,0:T(8,128)S(1)} %get-tuple-element.14.up_in, bf16[2048,256]{1,0:T(8,128)(2,1)S(1)} %bitcast.11, ...), custom_call_target="tpu_custom_call" | custom-call | tf_op jit(solution)/shard_map/expert/pallas_call | solution.py:148
  29.2 1.9 %collective-permute-start.1 = (bf16[256,1024]{1,0:T(8,128)(2,1)S(1)}, bf16[256,1024]{1,0:T(8,128)(2,1)S(1)}, u32[]{:S(2)}, u32[]{:S(2)}) collective-permute-start(bf16[256,1024]{1,0:T(8,128)(2,1)S(1)} %get-tuple-element.16), channel_id=1, source_target_pairs={{0,1},{1,0},{2,3},{3,2},{4,5},{5,4},{6,7},{7,6},{8,9},{9,8},{10,11... | collective-permute-start | bytes 1572872 | tf_op jit(solution)/shard_map/ppermute | solution.py:154
  31.2 1.9 %collective-permute-done.1 = bf16[256,1024]{1,0:T(8,128)(2,1)S(1)} collective-permute-done((bf16[256,1024]{1,0:T(8,128)(2,1)S(1)}, bf16[256,1024]{1,0:T(8,128)(2,1)S(1)}, u32[]{:S(2)}, u32[]{:S(2)}) %collective-permute-start.1) | collective-permute-done | bytes 524320 | tf_op jit(solution)/shard_map/ppermute | solution.py:154
  33.0 0.1 add_convert_fusion
  33.2 13.5 %all_to_all.16 = bf16[16,16,1024]{2,1,0:T(8,128)(2,1)S(1)} all-to-all(bf16[16,16,1024]{2,1,0:T(8,128)(2,1)S(1)} %bitcast.22), channel_id=1, replica_groups=mesh['ep'=16,'z'=16,'c'=2] {'ep'}, dimensions={0} | all-to-all | bytes 1048576 | tf_op jit(solution)/shard_map/all_to_all | solution.py:156
  46.7 0.3 combine.1
  47.0 26.3 %all_to_all.17.parts_ref = bf16[16,16,128]{2,1,0:T(8,128)(2,1)S(1)} all-to-all(bf16[16,16,128]{2,1,0:T(8,128)(2,1)S(1)} %combine.1), channel_id=1, replica_groups=mesh['ep'=16,'z'=16,'c'=2] {'z'}, dimensions={0} | all-to-all | bytes 131072 | tf_op jit(solution)/shard_map/all_to_all | solution.py:165
  73.3 0.7 total.1
Async XLA Ops:
  0.0 25.4 %copy-start = (bf16[1,2048,256]{2,1,0:T(8,128)(2,1)S(1)}, bf16[1,2048,256]{2,1,0:T(8,128)(2,1)}, u32[]{:S(2)}) copy-start(bf16[1,2048,256]{2,1,0:T(8,128)(2,1)} %param.11) | copy-start | bytes 3145732
  0.0 1.0 %copy-start.4 = (bf16[32,2048]{1,0:T(8,128)(2,1)S(1)}, bf16[32,2048]{1,0:T(8,128)(2,1)}, u32[]{:S(2)}) copy-start(bf16[32,2048]{1,0:T(8,128)(2,1)} %tok_ref.1) | copy-start | bytes 393220
  1.0 0.7 copy-start.5
  1.7 0.7 copy-start.6
  2.4 0.7 copy-start.7
  20.6 6.5 %collective-permute-start = (bf16[256,1024]{1,0:T(8,128)(2,1)S(1)}, bf16[256,1024]{1,0:T(8,128)(2,1)S(1)}, u32[]{:S(2)}, u32[]{:S(2)}) collective-permute-start(bf16[256,1024]{1,0:T(8,128)(2,1)S(1)} %bitcast.14), channel_id=1, source_target_pairs={{0,1},{1,0},{2,3},{3,2},{4,5},{5,4},{6,7},{7,6},{8,9},{9,8},{10,11... | collective-permute-start | bytes 1572872 | tf_op jit(solution)/shard_map/ppermute | solution.py:141
  25.4 1.2 %copy-start.1 = (bf16[1,2048,256]{2,1,0:T(8,128)(2,1)S(1)}, bf16[1,2048,256]{2,1,0:T(8,128)(2,1)}, u32[]{:S(2)}) copy-start(bf16[1,2048,256]{2,1,0:T(8,128)(2,1)} %param.12) | copy-start | bytes 3145732
  26.7 1.2 %copy-start.2 = (bf16[1,2048,256]{2,1,0:T(8,128)(2,1)S(1)}, bf16[1,2048,256]{2,1,0:T(8,128)(2,1)}, u32[]{:S(2)}) copy-start(bf16[1,2048,256]{2,1,0:T(8,128)(2,1)} %param.12) | copy-start | bytes 3145732
  26.7 1.5 %copy-start.3 = (bf16[1,256,2048]{2,1,0:T(8,128)(2,1)S(1)}, bf16[1,256,2048]{2,1,0:T(8,128)(2,1)}, u32[]{:S(2)}) copy-start(bf16[1,256,2048]{2,1,0:T(8,128)(2,1)} %param.13) | copy-start | bytes 3145732
  29.2 3.8 %collective-permute-start.1 = (bf16[256,1024]{1,0:T(8,128)(2,1)S(1)}, bf16[256,1024]{1,0:T(8,128)(2,1)S(1)}, u32[]{:S(2)}, u32[]{:S(2)}) collective-permute-start(bf16[256,1024]{1,0:T(8,128)(2,1)S(1)} %get-tuple-element.16), channel_id=1, source_target_pairs={{0,1},{1,0},{2,3},{3,2},{4,5},{5,4},{6,7},{7,6},{8,9},{9,8},{10,11... | collective-permute-start | bytes 1572872 | tf_op jit(solution)/shard_map/ppermute | solution.py:154

commit v2 on v1

--- a/solution.py
+++ b/solution.py
@@ -26,64 +26,110 @@
     return jnp.sum(jnp.where(eye, row, 0), axis=1, keepdims=True)
 
 
-def dispatch_kernel(tok_ref, gain_ref, picks_ref, weight_ref, buffer_ref, combine_ref):
-    rows, width = tok_ref.shape
+def in_hbm(*arrays):
+    return [pltpu.with_memory_space_constraint(x, pltpu.HBM) for x in arrays]
+
+
+def started(sems, *pairs):
+    copies = [pltpu.make_async_copy(src, dst, sems.at[i]) for i, (src, dst) in enumerate(pairs)]
+    for copy in copies:
+        copy.start()
+    return copies
+
+
+def dispatch_kernel(
+    tok_hbm,
+    gain_hbm,
+    picks_hbm,
+    weight_hbm,
+    gate_hbm,
+    up_hbm,
+    down_hbm,
+    buffer_ref,
+    combine_ref,
+    gate_ref,
+    up_ref,
+    down_ref,
+    tok,
+    gain,
+    picks,
+    weight,
+    sems,
+):
+    rows, width = tok.shape
     slots = buffer_ref.shape[0]
     cap = rows // 2
     part = width // 2
-    first = pl.multiple_of(lax.axis_index("c") * part, part)
-    values = tok_ref[...].astype(F32)
-    scale = lax.rsqrt(jnp.mean(values * values, axis=-1, keepdims=True) + 1e-06)
-    mine = tok_ref[:, pl.ds(first, part)].astype(F32)
-    normed = (mine * scale * gain_ref[:, pl.ds(first, part)]).astype(BF16)
+    core = lax.axis_index("c")
+    first = pl.multiple_of(core * part, part)
+    second = pl.multiple_of((1 - core) * part, part)
+    copies = started(
+        sems,
+        (picks_hbm, picks),
+        (weight_hbm, weight),
+        (tok_hbm, tok),
+        (gain_hbm, gain),
+        (gate_hbm.at[pl.ds(second, part), :], gate_ref),
+        (up_hbm.at[pl.ds(second, part), :], up_ref),
+        (down_hbm, down_ref),
+    )
 
     at_row = lax.broadcasted_iota(jnp.int32, (rows, rows), 0)
     at_col = lax.broadcasted_iota(jnp.int32, (rows, rows), 1)
     eye = at_row == at_col
     earlier = (at_col < at_row).astype(F32).astype(BF16)
-    pick0 = column(picks_ref[0:1, :], eye)
-    pick1 = column(picks_ref[1:2, :], eye)
-    weight0 = column(weight_ref[0:1, :], eye)
-    weight1 = column(weight_ref[1:2, :], eye)
     slot = lax.broadcasted_iota(jnp.int32, (rows, slots), 1)
     expert = slot // cap
     place = (slot % cap).astype(F32)
+    copies[0].wait()
+    copies[1].wait()
+    pick0 = column(picks[0:1, :], eye)
+    pick1 = column(picks[1:2, :], eye)
+    weight0 = column(weight[0:1, :], eye)
+    weight1 = column(weight[1:2, :], eye)
     is0 = pick0 == expert
     is1 = pick1 == expert
     chosen = (is0 | is1).astype(F32)
     rank = jnp.dot(earlier, chosen.astype(BF16), preferred_element_type=F32)
     table = jnp.where(rank == place, chosen, 0.0)
-    buffer_ref[...] = jnp.dot(
-        table.T.astype(BF16), normed, preferred_element_type=F32
-    ).astype(BF16)
     weights = table * jnp.where(is0, weight0, weight1)
     high = weights.astype(BF16)
     combine_ref[0:rows, :] = high
     combine_ref[rows:, :] = (weights - high.astype(F32)).astype(BF16)
-
-
-def first_half_kernel(rows_ref, gate_ref, up_ref, gate_out, up_out):
+    spread = table.T.astype(BF16)
+
+    copies[2].wait()
+    copies[3].wait()
+    values = tok[...].astype(F32)
+    scale = lax.rsqrt(jnp.mean(values * values, axis=-1, keepdims=True) + 1e-06)
+    mine = tok[:, pl.ds(first, part)].astype(F32)
+    normed = (mine * scale * gain[:, pl.ds(first, part)]).astype(BF16)
+    buffer_ref[...] = jnp.dot(spread, normed, preferred_element_type=F32).astype(BF16)
+    for copy in copies[4:]:
+        copy.wait()
+
+
+def first_half_kernel(rows_ref, gate_hbm, up_hbm, gate_out, up_out, gate, up, sems):
     part = rows_ref.shape[1]
     first = pl.multiple_of(lax.axis_index("c") * part, part)
+    copies = started(
+        sems, (gate_hbm.at[pl.ds(first, part), :], gate), (up_hbm.at[pl.ds(first, part), :], up)
+    )
     rows = rows_ref[...]
-    gate_out[...] = jnp.dot(rows, gate_ref[pl.ds(first, part), :], preferred_element_type=F32)
-    up_out[...] = jnp.dot(rows, up_ref[pl.ds(first, part), :], preferred_element_type=F32)
+    copies[0].wait()
+    gate_out[...] = jnp.dot(rows, gate[...], preferred_element_type=F32)
+    copies[1].wait()
+    up_out[...] = jnp.dot(rows, up[...], preferred_element_type=F32)
 
 
 def expert_kernel(rows_ref, gate_in, up_in, gate_ref, up_ref, down_ref, mine_out, send_out):
-    part = rows_ref.shape[1]
-    core = lax.axis_index("c")
-    first = pl.multiple_of((1 - core) * part, part)
     rows = rows_ref[...]
-    gate = gate_in[...] + jnp.dot(
-        rows, gate_ref[pl.ds(first, part), :], preferred_element_type=F32
-    )
-    upper = up_in[...] + jnp.dot(rows, up_ref[pl.ds(first, part), :], preferred_element_type=F32)
+    gate = gate_in[...] + jnp.dot(rows, gate_ref[...], preferred_element_type=F32)
+    upper = up_in[...] + jnp.dot(rows, up_ref[...], preferred_element_type=F32)
     hidden = (gate / (1.0 + jnp.exp(-gate)) * upper).astype(BF16)
-    is_low = core == 0
+    is_low = lax.axis_index("c") == 0
     lane = lax.broadcasted_iota(jnp.int32, (rows.shape[0], LANES), 1)
-    low_lane = lane < HALF
-    stay = low_lane == is_low
+    stay = (lane < HALF) == is_low
     for m in range(mine_out.shape[1] // LANES):
         pair = jnp.dot(
             hidden, down_ref[:, 2 * m * LANES : 2 * (m + 1) * LANES], preferred_element_type=F32
@@ -129,28 +175,53 @@
     w_gate, w_up, w_down = expert_gate[0], expert_up[0], expert_down[0]
     units = w_gate.shape[1]
 
-    buffer, table = pl.pallas_call(
+    gain = norm_gain[None, :]
+    picks = routes.T
+    weights = gate_weights.T
+    hbm = pl.BlockSpec(memory_space=pltpu.HBM)
+    vmem = pl.BlockSpec(memory_space=pltpu.VMEM)
+    buffer, table, gate_rest, up_rest, down = pl.pallas_call(
         dispatch_kernel,
-        out_shape=(shape((slots, part), BF16), shape((2 * rows, slots), BF16)),
+        in_specs=[hbm] * 7,
+        out_shape=(
+            shape((slots, part), BF16),
+            shape((2 * rows, slots), BF16),
+            shape((part, units), BF16),
+            shape((part, units), BF16),
+            shape(w_down.shape, BF16),
+        ),
+        scratch_shapes=[
+            pltpu.VMEM(tokens.shape, tokens.dtype),
+            pltpu.VMEM(gain.shape, gain.dtype),
+            pltpu.VMEM(picks.shape, picks.dtype),
+            pltpu.VMEM(weights.shape, weights.dtype),
+            pltpu.SemaphoreType.DMA((7,)),
+        ],
         compiler_params=params(8),
         name="dispatch",
-    )(tokens, norm_gain[None, :], routes.T, gate_weights.T)
+    )(*in_hbm(tokens, gain, picks, weights, w_gate, w_up, w_down))
     received = lax.all_to_all(
         buffer.reshape(n_ep, cap, part), "ep", split_axis=0, concat_axis=0, tiled=True
     ).reshape(slots, part)
     other = lax.ppermute(received, "c", SWAP)
     gate, upper = pl.pallas_call(
         first_half_kernel,
+        in_specs=[vmem, hbm, hbm],
         out_shape=(shape((slots, units), F32), shape((slots, units), F32)),
+        scratch_shapes=[
+            pltpu.VMEM((part, units), BF16),
+            pltpu.VMEM((part, units), BF16),
+            pltpu.SemaphoreType.DMA((2,)),
+        ],
         compiler_params=params(8),
         name="first_half",
-    )(received, w_gate, w_up)
+    )(received, *in_hbm(w_gate, w_up))
     mine, send = pl.pallas_call(
         expert_kernel,
         out_shape=(shape((slots, part), F32), shape((slots, part), BF16)),
         compiler_params=params(12),
         name="expert",
-    )(other, gate, upper, w_gate, w_up, w_down)
+    )(other, gate, upper, gate_rest, up_rest, down)
     arrived = lax.ppermute(send, "c", SWAP)
     outputs = (mine + arrived.astype(F32)).astype(BF16)
     back = lax.all_to_all(

time: 75.2 us -> 72.3 us (0.961)
  local copies, waits for them, and re-layouts: 5.36 us -> 0 us
  Pallas kernels: 2.99 us -> 5.64 us
    unnamed x16 -> x0, local copies, waits for them, and re-layouts: 5.36 us -> none
    pallas_call x2, Pallas kernels: 0.98 us -> 3.63 us  [the longest x1 1.91 us: shards(): pl.pallas_call(first_half_kernel, in_specs=[vmem, hbm, hbm], out_shape=(s...]
  transfers between devices with their start and end apart: 2 -> 2, of which waited for: 1 -> 1; matrix products, arithmetic and copies ran while one was open for 0% -> 0% of each run, Pallas kernels for 1% -> 3%
where the time goes in v2:
time: 72.3 us; the launch traced here: 71.3 us
  blocking collectives  56.8 us (79%)
  starting transfers between devices  6.71 us (9%)
  Pallas kernels  5.64 us (8%)
  waiting for transfers between devices  1.88 us (3%)
    all_to_all x1, blocking collectives, shards(): parts = lax.all_to_all(packed, 'z', split_axis=0, concat_axis=0, tiled=True)  26.3 us
    all_to_all x1, blocking collectives, shards(): lax.all_to_all(buffer.reshape(n_ep, cap, part), 'ep', split_axis=0, conca...  17 us
    all_to_all x1, blocking collectives, shards(): lax.all_to_all(outputs.reshape(n_ep, cap, part), 'ep', split_axis=0, conc...  13.5 us
    ppermute x1, starting transfers between devices, shards(): other = lax.ppermute(received, 'c', SWAP)  4.79 us
    ppermute x1, starting transfers between devices, shards(): arrived = lax.ppermute(send, 'c', SWAP)  1.92 us
    pallas_call x1, Pallas kernels, shards(): pl.pallas_call(first_half_kernel, in_specs=[vmem, hbm, hbm], out_shape=(s...  1.91 us
    ppermute x1, waiting for transfers between devices, shards(): arrived = lax.ppermute(send, 'c', SWAP)  1.88 us
    pallas_call x1, Pallas kernels, shards(): pl.pallas_call(dispatch_kernel, in_specs=[hbm] * 7, out_shape=(shape((slo...  1.72 us
  transfers between devices with their start and end apart: 2, of which 1 were waited for; matrix products, arithmetic and copies ran while one was open for 0% of the time, Pallas kernels for 3%

profile of v2, /device:TPU:1, one launch (start us, length us, event | category | flops | bytes accessed | tf_op | source)
XLA Modules:
  0.0 71.3 jit_solution(1028658329282508208)
XLA Ops:
  0.0 1.7 %dispatch.1 = (bf16[256,1024]{1,0:T(8,128)(2,1)S(1)}, bf16[64,256]{1,0:T(8,128)(2,1)S(1)}, bf16[1024,256]{1,0:T(8,128)(2,1)S(1)}, bf16[1024,256]{1,0:T(8,128)(2,1)S(1)}, bf16[256,2048]{1,0:T(8,128)(2,1)S(1)}) custom-call(bf16[32,2048]{1,0:T(8,128)(2,1)} %tok_hbm.1, f32[1,2048]{1,0:T(1,128)} %bitcast.20, s32[2,32]{1,0:T(2,128)} %bitcast.21, ...), custom_call_target="tpu_custom_call" | custom-call | tf_op jit(solution)/shard_map/dispatch/pallas_call | solution.py:183
  1.7 17.0 %all_to_all.15 = bf16[16,16,1024]{2,1,0:T(8,128)(2,1)S(1)} all-to-all(bf16[16,16,1024]{2,1,0:T(8,128)(2,1)S(1)} %bitcast.13), channel_id=1, replica_groups=mesh['ep'=16,'z'=16,'c'=2] {'ep'}, dimensions={0} | all-to-all | bytes 1048576 | tf_op jit(solution)/shard_map/all_to_all | solution.py:203
  18.7 4.8 %collective-permute-start = (bf16[256,1024]{1,0:T(8,128)(2,1)S(1)}, bf16[256,1024]{1,0:T(8,128)(2,1)S(1)}, u32[]{:S(2)}, u32[]{:S(2)}) collective-permute-start(bf16[256,1024]{1,0:T(8,128)(2,1)S(1)} %bitcast.10), channel_id=1, source_target_pairs={{0,1},{1,0},{2,3},{3,2},{4,5},{5,4},{6,7},{7,6},{8,9},{9,8},{10,11... | collective-permute-start | bytes 1572872 | tf_op jit(solution)/shard_map/ppermute | solution.py:206
  23.5 1.9 %first_half.1 = (f32[256,256]{1,0:T(8,128)S(1)}, f32[256,256]{1,0:T(8,128)S(1)}) custom-call(bf16[256,1024]{1,0:T(8,128)(2,1)S(1)} %bitcast.11, bf16[2048,256]{1,0:T(8,128)(2,1)} %bitcast.15, bf16[2048,256]{1,0:T(8,128)(2,1)} %bitcast.17), custom_call_target="tpu_custom_call" | custom-call | tf_op jit(solution)/shard_map/first_half/pallas_call | solution.py:207
  25.5 0.0 collective-permute-done.rows_ref
  25.5 1.0 %expert.1 = (f32[256,1024]{1,0:T(8,128)S(1)}, bf16[256,1024]{1,0:T(8,128)(2,1)S(1)}) custom-call(bf16[256,1024]{1,0:T(8,128)(2,1)S(1)} %collective-permute-done.rows_ref, f32[256,256]{1,0:T(8,128)S(1)} %get-tuple-element.16.gate_in, f32[256,256]{1,0:T(8,128)S(1)} %get-tuple-element.17.up_in, bf16[1024,256]{1,0:T(8,128)(2,1)S(1)} %get-tuple-element.18.gate_ref, ...), custom_call_target="tpu_custom_call" | custom-call | tf_op jit(solution)/shard_map/expert/pallas_call | solution.py:219
  26.5 1.9 %collective-permute-start.1 = (bf16[256,1024]{1,0:T(8,128)(2,1)S(1)}, bf16[256,1024]{1,0:T(8,128)(2,1)S(1)}, u32[]{:S(2)}, u32[]{:S(2)}) collective-permute-start(bf16[256,1024]{1,0:T(8,128)(2,1)S(1)} %get-tuple-element.22), channel_id=1, source_target_pairs={{0,1},{1,0},{2,3},{3,2},{4,5},{5,4},{6,7},{7,6},{8,9},{9,8},{10,11... | collective-permute-start | bytes 1572872 | tf_op jit(solution)/shard_map/ppermute | solution.py:225
  28.4 1.9 %collective-permute-done.1 = bf16[256,1024]{1,0:T(8,128)(2,1)S(1)} collective-permute-done((bf16[256,1024]{1,0:T(8,128)(2,1)S(1)}, bf16[256,1024]{1,0:T(8,128)(2,1)S(1)}, u32[]{:S(2)}, u32[]{:S(2)}) %collective-permute-start.1) | collective-permute-done | bytes 524320 | tf_op jit(solution)/shard_map/ppermute | solution.py:225
  30.3 0.1 add_convert_fusion
  30.5 13.5 %all_to_all.16 = bf16[16,16,1024]{2,1,0:T(8,128)(2,1)S(1)} all-to-all(bf16[16,16,1024]{2,1,0:T(8,128)(2,1)S(1)} %bitcast.18), channel_id=1, replica_groups=mesh['ep'=16,'z'=16,'c'=2] {'ep'}, dimensions={0} | all-to-all | bytes 1048576 | tf_op jit(solution)/shard_map/all_to_all | solution.py:227
  44.0 0.3 combine.1
  44.3 26.3 %all_to_all.17.parts_ref = bf16[16,16,128]{2,1,0:T(8,128)(2,1)S(1)} all-to-all(bf16[16,16,128]{2,1,0:T(8,128)(2,1)S(1)} %combine.1), channel_id=1, replica_groups=mesh['ep'=16,'z'=16,'c'=2] {'z'}, dimensions={0} | all-to-all | bytes 131072 | tf_op jit(solution)/shard_map/all_to_all | solution.py:236
  70.6 0.7 total.1
Async XLA Ops:
  18.7 6.7 %collective-permute-start = (bf16[256,1024]{1,0:T(8,128)(2,1)S(1)}, bf16[256,1024]{1,0:T(8,128)(2,1)S(1)}, u32[]{:S(2)}, u32[]{:S(2)}) collective-permute-start(bf16[256,1024]{1,0:T(8,128)(2,1)S(1)} %bitcast.10), channel_id=1, source_target_pairs={{0,1},{1,0},{2,3},{3,2},{4,5},{5,4},{6,7},{7,6},{8,9},{9,8},{10,11... | collective-permute-start | bytes 1572872 | tf_op jit(solution)/shard_map/ppermute | solution.py:206
  26.5 3.8 %collective-permute-start.1 = (bf16[256,1024]{1,0:T(8,128)(2,1)S(1)}, bf16[256,1024]{1,0:T(8,128)(2,1)S(1)}, u32[]{:S(2)}, u32[]{:S(2)}) collective-permute-start(bf16[256,1024]{1,0:T(8,128)(2,1)S(1)} %get-tuple-element.22), channel_id=1, source_target_pairs={{0,1},{1,0},{2,3},{3,2},{4,5},{5,4},{6,7},{7,6},{8,9},{9,8},{10,11... | collective-permute-start | bytes 1572872 | tf_op jit(solution)/shard_map/ppermute | solution.py:225

commit v3 on v2

v3 whole, which is shorter than its diff:
```python
import jax
import jax.numpy as jnp
import numpy as np
from jax import lax
from jax.experimental import pallas as pl
from jax.experimental.pallas import tpu as pltpu
from jax.sharding import Mesh
from jax.sharding import PartitionSpec as P


LANES = 128
HALF = LANES // 2
F32 = jnp.float32
BF16 = jnp.bfloat16
SWAP = ((0, 1), (1, 0))


def params(mib):
    return pltpu.CompilerParams(vmem_limit_bytes=mib * 2**20)


def flipped(x):
    return pltpu.roll(x, HALF, axis=x.ndim - 1)


def column(row, eye):
    return jnp.sum(jnp.where(eye, row, 0), axis=1, keepdims=True)


def in_hbm(*arrays):
    return [pltpu.with_memory_space_constraint(x, pltpu.HBM) for x in arrays]


def started(sems, *pairs):
    copies = [pltpu.make_async_copy(src, dst, sems.at[i]) for i, (src, dst) in enumerate(pairs)]
    for copy in copies:
        copy.start()
    return copies


def dispatch_kernel(
    tok_hbm,
    gain_hbm,
    picks_hbm,
    weight_hbm,
    buffer_hbm,
    combine_ref,
    tok,
    gain,
    picks,
    weight,
    buffer,
    sems,
    out_sems,
):
    copies = started(
        sems, (tok_hbm, tok), (gain_hbm, gain), (picks_hbm, picks), (weight_hbm, weight)
    )
    rows, width = tok.shape
    slots = combine_ref.shape[1]
    cap = rows // 2
    core = lax.axis_index("c")

    at_row = lax.broadcasted_iota(jnp.int32, (rows, rows), 0)
    at_col = lax.broadcasted_iota(jnp.int32, (rows, rows), 1)
    eye = at_row == at_col
    earlier = (at_col < at_row).astype(F32).astype(BF16)
    copies[2].wait()
    copies[3].wait()
    pick0 = column(picks[0:1, :], eye)
    pick1 = column(picks[1:2, :], eye)
    weight0 = column(weight[0:1, :], eye)
    weight1 = column(weight[1:2, :], eye)

    def placed(count, each, base):
        slot = lax.broadcasted_iota(jnp.int32, (rows, count), 1)
        expert = slot // each
        is0 = pick0 == expert
        chosen = (is0 | (pick1 == expert)).astype(F32)
        rank = jnp.dot(earlier, chosen.astype(BF16), preferred_element_type=F32)
        place = (slot % each + base).astype(F32)
        return jnp.where(rank == place, chosen, 0.0), is0

    mine, _ = placed(slots // 2, cap // 2, core * (cap // 2))
    spread = mine.T.astype(BF16)
    table, is0 = placed(slots, cap, 0)
    weights = table * jnp.where(is0, weight0, weight1)
    high = weights.astype(BF16)
    combine_ref[0:rows, :] = high
    combine_ref[rows:, :] = (weights - high.astype(F32)).astype(BF16)

    copies[0].wait()
    copies[1].wait()
    values = tok[...].astype(F32)
    scale = lax.rsqrt(jnp.mean(values * values, axis=-1, keepdims=True) + 1e-06)
    chunks = out_sems.shape[0]
    leaving = []
    for i in range(chunks):
        at = pl.ds(i * (width // chunks), width // chunks)
        normed = (tok[:, at].astype(F32) * scale * gain[:, at]).astype(BF16)
        buffer[:, at] = jnp.dot(spread, normed, preferred_element_type=F32).astype(BF16)
        leaving.append(
            pltpu.make_async_copy(buffer.at[:, at], buffer_hbm.at[:, at], out_sems.at[i])
        )
        leaving[-1].start()
    for copy in leaving:
        copy.wait()


def load_kernel(src_hbm, dst, sems):
    (copy,) = started(sems, (src_hbm.at[pl.ds(0, dst.shape[0]), :], dst))
    copy.wait()


def times(a, w):
    return jnp.dot(a, w[...], preferred_element_type=F32)


def hidden_of(gate, upper):
    return (gate / (1.0 + jnp.exp(-gate)) * upper).astype(BF16)


def hidden_kernel(
    rows_ref,
    head0,
    gate0_hbm,
    up0_hbm,
    gate1_hbm,
    down0_hbm,
    hidden0_ref,
    gate1_out,
    down0_ref,
    tail0,
    up0,
    gate1,
    sems,
):
    cut = head0.shape[0]
    copies = started(
        sems,
        (gate0_hbm.at[pl.ds(cut, tail0.shape[0]), :], tail0),
        (up0_hbm, up0),
        (gate1_hbm, gate1),
        (down0_hbm, down0_ref),
    )
    gate = times(rows_ref[:, :cut], head0)
    copies[0].wait()
    gate = gate + times(rows_ref[:, cut:], tail0)
    copies[1].wait()
    hidden0_ref[...] = hidden_of(gate, times(rows_ref[...], up0))
    copies[2].wait()
    gate1_out[...] = times(rows_ref[...], gate1)
    copies[3].wait()


def down_kernel(rows_ref, up1, gate1_in, hidden0_ref, down0_ref, down1_ref, out_ref):
    n_ep, _, cap, part = out_ref.shape
    hidden0 = hidden0_ref[...]
    hidden1 = hidden_of(gate1_in[...], times(rows_ref[...], up1))
    low_lane = lax.broadcasted_iota(jnp.int32, (n_ep * cap, LANES), 1) < HALF
    for m in range(part // LANES):
        pair = slice(2 * m * LANES, 2 * (m + 1) * LANES)
        out = times(hidden0, down0_ref.at[:, pair]) + times(hidden1, down1_ref.at[:, pair])
        a, b = out[:, :LANES], out[:, LANES:]
        at = slice(m * LANES, (m + 1) * LANES)
        low = jnp.where(low_lane, a, flipped(b)).astype(BF16)
        high = jnp.where(low_lane, flipped(a), b).astype(BF16)
        out_ref[:, 0, :, at] = low.reshape(n_ep, cap, LANES)
        out_ref[:, 1, :, at] = high.reshape(n_ep, cap, LANES)


def combine_kernel(table_ref, back_ref, out_ref):
    rows = table_ref.shape[0] // 2
    half = rows // 2
    both = jnp.dot(table_ref[...], back_ref[...], preferred_element_type=F32)
    mixed = both[:rows] + both[rows:]
    low_lane = lax.broadcasted_iota(jnp.int32, (half, LANES), 1) < HALF
    for m in range(back_ref.shape[1] // LANES):
        at = slice(m * LANES, (m + 1) * LANES)
        a, b = mixed[:half, at], mixed[half:, at]
        out_ref[2 * m] = jnp.where(low_lane, a, flipped(b)).astype(BF16)
        out_ref[2 * m + 1] = jnp.where(low_lane, flipped(a), b).astype(BF16)


def total_kernel(parts_ref, out_ref):
    half = out_ref.shape[0] // 2
    total = jnp.sum(parts_ref[...].astype(F32), axis=0)
    out_ref[:half, :] = total[:, :HALF].astype(BF16)
    out_ref[half:, :] = flipped(total)[:, :HALF].astype(BF16)


def shape(dims, dtype):
    return jax.ShapeDtypeStruct(dims, dtype)


def shards(tokens, norm_gain, routes, gate_weights, expert_gate, expert_up, expert_down):
    rows, width = tokens.shape
    n_ep = lax.axis_size("ep")
    n_z = lax.axis_size("z")
    cap = rows // 2
    each = cap // 2
    slots = n_ep * cap
    mine = slots // 2
    part = width // 2
    w_gate, w_up, w_down = expert_gate[0], expert_up[0], expert_down[0]
    units = w_gate.shape[1]

    gain = norm_gain[None, :]
    picks = routes.T
    weights = gate_weights.T
    hbm = pl.BlockSpec(memory_space=pltpu.HBM)
    vmem = pl.BlockSpec(memory_space=pltpu.VMEM)
    buffer, table = pl.pallas_call(
        dispatch_kernel,
        in_specs=[hbm] * 4,
        out_shape=(shape((mine, width), BF16), shape((2 * rows, slots), BF16)),
        out_specs=(hbm, vmem),
        scratch_shapes=[
            pltpu.VMEM(tokens.shape, tokens.dtype),
            pltpu.VMEM(gain.shape, gain.dtype),
            pltpu.VMEM(picks.shape, picks.dtype),
            pltpu.VMEM(weights.shape, weights.dtype),
            pltpu.VMEM((mine, width), BF16),
            pltpu.SemaphoreType.DMA((4,)),
            pltpu.SemaphoreType.DMA((4,)),
        ],
        compiler_params=params(8),
        name="dispatch",
    )(*in_hbm(tokens, gain, picks, weights))
    received = lax.all_to_all(
        buffer.reshape(n_ep, each, width), "ep", split_axis=0, concat_axis=0, tiled=True
    ).reshape(mine, width)
    o_down = lax.ppermute(w_down, "c", SWAP)
    o_gate = lax.ppermute(w_gate, "c", SWAP)
    o_up = lax.ppermute(w_up, "c", SWAP)
    cut = width * 3 // 4
    head = pl.pallas_call(
        load_kernel,
        in_specs=[hbm],
        out_shape=shape((cut, units), BF16),
        scratch_shapes=[pltpu.SemaphoreType.DMA((1,))],
        compiler_params=params(8),
        name="load",
    )(*in_hbm(w_gate))
    hidden0, gate1, down = pl.pallas_call(
        hidden_kernel,
        in_specs=[vmem] * 2 + [hbm] * 4,
        out_shape=(
            shape((mine, units), BF16),
            shape((mine, units), F32),
            shape(w_down.shape, BF16),
        ),
        scratch_shapes=[
            pltpu.VMEM((width - cut, units), BF16),
            pltpu.VMEM(w_up.shape, BF16),
            pltpu.VMEM(w_gate.shape, BF16),
            pltpu.SemaphoreType.DMA((4,)),
        ],
        compiler_params=params(8),
        name="hidden",
    )(received, head, *in_hbm(w_gate, w_up, o_gate, w_down))
    outputs = pl.pallas_call(
        down_kernel,
        out_shape=shape((n_ep, 2, each, part), BF16),
        compiler_params=params(8),
        name="down",
    )(received, o_up, gate1, hidden0, down, o_down)
    back = lax.all_to_all(
        outputs.reshape(2 * n_ep, each, part), ("ep", "c"), split_axis=0, concat_axis=0, tiled=True
    ).reshape(slots, part)
    packed = pl.pallas_call(
        combine_kernel,
        out_shape=shape((n_z, rows // 2, LANES), BF16),
        compiler_params=params(8),
        name="combine",
    )(table, back)
    parts = lax.all_to_all(packed, "z", split_axis=0, concat_axis=0, tiled=True)
    return pl.pallas_call(
        total_kernel,
        out_shape=shape((rows, HALF), BF16),
        compiler_params=params(8),
        name="total",
    )(parts)


def solution(mesh):
    n_ep, n_tp = mesh.devices.shape
    chips = Mesh(np.asarray(mesh.devices).reshape(n_ep, n_tp // 2, 2), ("ep", "z", "c"))
    tp = ("z", "c")
    placed = (
        P("ep", None),
        P(),
        P("ep", None),
        P("ep", None),
        P("ep", None, tp),
        P("ep", None, tp),
        P("ep", tp, None),
    )
    return jax.shard_map(
        shards, mesh=chips, in_specs=placed, out_specs=P("ep", tp), check_vma=False
    )
```

time: 72.3 us -> 74.6 us (1.032)
  blocking collectives: 56.8 us -> 39.7 us
  starting transfers between devices: 6.71 us -> 16.7 us
  waiting for transfers between devices: 1.88 us -> 10.2 us
  Pallas kernels: 5.64 us -> 7.59 us
    all_to_all x2 -> x1, blocking collectives: 30.6 us -> 15.7 us  [shards(): lax.all_to_all(outputs.reshape(2 * n_ep, each, part), ('ep', 'c'), split_...]
    all_to_all x0 -> x1, waiting for transfers between devices: none -> 10.1 us  [shards(): lax.all_to_all(buffer.reshape(n_ep, each, width), 'ep', split_axis=0, con...]
    ppermute x2 -> x3, starting transfers between devices: 6.71 us -> 13.1 us  [the longest x1 8.74 us: shards(): o_gate = lax.ppermute(w_gate, 'c', SWAP)]
    all_to_all x0 -> x1, starting transfers between devices: none -> 3.58 us  [shards(): lax.all_to_all(buffer.reshape(n_ep, each, width), 'ep', split_axis=0, con...]
    all_to_all x1, blocking collectives: 26.3 us -> 24 us  [shards(): parts = lax.all_to_all(packed, 'z', split_axis=0, concat_axis=0, tiled=True)]
    pallas_call x3 -> x4, Pallas kernels: 4.67 us -> 6.62 us  [the longest x1 2.27 us: shards(): pl.pallas_call(dispatch_kernel, in_specs=[hbm] * 4, out_shape=(shape((min...]
    ppermute x2 -> x3, waiting for transfers between devices: 1.88 us -> 0.01 us  [the longest x1 0.01 us: shards(): o_gate = lax.ppermute(w_gate, 'c', SWAP)]
  transfers between devices with their start and end apart: 2 -> 4, of which waited for: 1 -> 1; matrix products, arithmetic and copies ran while one was open for 0% -> 0% of each run, Pallas kernels for 3% -> 8%
where the time goes in v3:
time: 74.6 us; the launch traced here: 74.2 us
  blocking collectives  39.7 us (53%)
  starting transfers between devices  16.7 us (22%)
  waiting for transfers between devices  10.2 us (14%)
  Pallas kernels  7.59 us (10%)
    all_to_all x1, blocking collectives, shards(): parts = lax.all_to_all(packed, 'z', split_axis=0, concat_axis=0, tiled=True)  24 us
    all_to_all x1, blocking collectives, shards(): lax.all_to_all(outputs.reshape(2 * n_ep, each, part), ('ep', 'c'), split_...  15.7 us
    all_to_all x1, waiting for transfers between devices, shards(): lax.all_to_all(buffer.reshape(n_ep, each, width), 'ep', split_axis=0, con...  10.1 us
    ppermute x1, starting transfers between devices, shards(): o_gate = lax.ppermute(w_gate, 'c', SWAP)  8.74 us
    all_to_all x1, starting transfers between devices, shards(): lax.all_to_all(buffer.reshape(n_ep, each, width), 'ep', split_axis=0, con...  3.58 us
    ppermute x1, starting transfers between devices, shards(): o_down = lax.ppermute(w_down, 'c', SWAP)  2.41 us
    pallas_call x1, Pallas kernels, shards(): pl.pallas_call(dispatch_kernel, in_specs=[hbm] * 4, out_shape=(shape((min...  2.27 us
    pallas_call x1, Pallas kernels, shards(): pl.pallas_call(hidden_kernel, in_specs=[vmem] * 2 + [hbm] * 4, out_shape=...  2.19 us
  transfers between devices with their start and end apart: 4, of which 1 were waited for; matrix products, arithmetic and copies ran while one was open for 0% of the time, Pallas kernels for 8%

profile of v3, /device:TPU:1, one launch (start us, length us, event | category | flops | bytes accessed | tf_op | source)
XLA Modules:
  0.0 74.2 jit_solution(10756276665953853300)
XLA Ops:
  0.0 8.7 %collective-permute-start.1 = (bf16[2048,256]{1,0:T(8,128)(2,1)}, bf16[2048,256]{1,0:T(8,128)(2,1)}, u32[]{:S(2)}, u32[]{:S(2)}) collective-permute-start(bf16[2048,256]{1,0:T(8,128)(2,1)} %bitcast.14), channel_id=1, source_target_pairs={{0,1},{1,0},{2,3},{3,2},{4,5},{5,4},{6,7},{7,6},{8,9},{9,8},{10,11... | collective-permute-start | bytes 3145736 | tf_op jit(solution)/shard_map/ppermute | solution.py:234
  8.7 1.9 %collective-permute-start = (bf16[2048,256]{1,0:T(8,128)(2,1)}, bf16[2048,256]{1,0:T(8,128)(2,1)S(1)}, u32[]{:S(2)}, u32[]{:S(2)}) collective-permute-start(bf16[2048,256]{1,0:T(8,128)(2,1)} %bitcast.17), channel_id=1, source_target_pairs={{0,1},{1,0},{2,3},{3,2},{4,5},{5,4},{6,7},{7,6},{8,9},{9,8},{10,11... | collective-permute-start | bytes 3145736 | tf_op jit(solution)/shard_map/ppermute | solution.py:235
  10.7 2.4 %collective-permute-start.2 = (bf16[256,2048]{1,0:T(8,128)(2,1)}, bf16[256,2048]{1,0:T(8,128)(2,1)S(1)}, u32[]{:S(2)}, u32[]{:S(2)}) collective-permute-start(bf16[256,2048]{1,0:T(8,128)(2,1)} %bitcast.19), channel_id=1, source_target_pairs={{0,1},{1,0},{2,3},{3,2},{4,5},{5,4},{6,7},{7,6},{8,9},{9,8},{10,11... | collective-permute-start | bytes 3145736 | tf_op jit(solution)/shard_map/ppermute | solution.py:233
  13.1 2.3 %dispatch.1 = (bf16[128,2048]{1,0:T(8,128)(2,1)}, bf16[64,256]{1,0:T(8,128)(2,1)S(1)}) custom-call(bf16[32,2048]{1,0:T(8,128)(2,1)} %tok_hbm.1, f32[1,2048]{1,0:T(1,128)} %bitcast.21, s32[2,32]{1,0:T(2,128)} %bitcast.22, f32[2,32]{1,0:T(2,128)} %bitcast.23), custom_call_target="tpu_custom_call" | custom-call | tf_op jit(solution)/shard_map/dispatch/pallas_call | solution.py:213
  15.4 3.6 %all-to-all-start = ((bf16[16,8,2048]{2,1,0:T(8,128)(2,1)}), bf16[16,8,2048]{2,1,0:T(8,128)(2,1)S(1)}, u32[]{:S(2)}, u32[]{:S(2)}) async-start(bf16[16,8,2048]{2,1,0:T(8,128)(2,1)} %bitcast.3), calls=%async_computation | async-start | bytes 1048576 | tf_op jit(solution)/shard_map/all_to_all | solution.py:230
  19.0 1.1 %load.1.head0 = bf16[1536,256]{1,0:T(8,128)(2,1)S(1)} custom-call(bf16[2048,256]{1,0:T(8,128)(2,1)} %bitcast.15), custom_call_target="tpu_custom_call" | custom-call | tf_op jit(solution)/shard_map/load/pallas_call | solution.py:237
  20.1 10.1 %all-to-all-done = bf16[16,8,2048]{2,1,0:T(8,128)(2,1)S(1)} async-done(((bf16[16,8,2048]{2,1,0:T(8,128)(2,1)}), bf16[16,8,2048]{2,1,0:T(8,128)(2,1)S(1)}, u32[]{:S(2)}, u32[]{:S(2)}) %all-to-all-start) | async-done | bytes 524320 | tf_op jit(solution)/shard_map/all_to_all | solution.py:230
  30.3 0.0 collective-permute-done.1.gate1_hbm
  30.3 2.2 %hidden.1 = (bf16[128,256]{1,0:T(8,128)(2,1)S(1)}, f32[128,256]{1,0:T(8,128)S(1)}, bf16[256,2048]{1,0:T(8,128)(2,1)S(1)}) custom-call(bf16[128,2048]{1,0:T(8,128)(2,1)S(1)} %bitcast.10, bf16[1536,256]{1,0:T(8,128)(2,1)S(1)} %load.1.head0, bf16[2048,256]{1,0:T(8,128)(2,1)} %bitcast.16, bf16[2048,256]{1,0:T(8,128)(2,1)} %bitcast.18, ...), custom_call_target="tpu_custom_call" | custom-call | tf_op jit(solution)/shard_map/hidden/pallas_call | solution.py:245
  32.5 0.0 collective-permute-done.up1
  32.5 0.0 collective-permute-done.2.down1_ref
  32.5 1.0 %down.1 = bf16[16,2,8,1024]{3,2,1,0:T(8,128)(2,1)S(1)} custom-call(bf16[128,2048]{1,0:T(8,128)(2,1)S(1)} %bitcast.11, bf16[2048,256]{1,0:T(8,128)(2,1)S(1)} %collective-permute-done.up1, f32[128,256]{1,0:T(8,128)S(1)} %get-tuple-element.12.gate1_in, bf16[128,256]{1,0:T(8,128)(2,1)S(1)} %get-tuple-element.13.hidden0_ref, ...), custom_call_target="tpu_custom_call" | custom-call | tf_op jit(solution)/shard_map/down/pallas_call | solution.py:262
  33.5 15.7 %all_to_all.15 = bf16[32,8,1024]{2,1,0:T(8,128)(2,1)S(1)} all-to-all(bf16[32,8,1024]{2,1,0:T(8,128)(2,1)S(1)} %bitcast.12), channel_id=1, replica_groups=mesh['ep'=16,'z'=16,'c'=2] {'ep','c'}, dimensions={0} | all-to-all | bytes 1048576 | tf_op jit(solution)/shard_map/all_to_all | solution.py:268
  49.2 0.3 combine.1
  49.5 24.0 %all_to_all.16.parts_ref = bf16[16,16,128]{2,1,0:T(8,128)(2,1)S(1)} all-to-all(bf16[16,16,128]{2,1,0:T(8,128)(2,1)S(1)} %combine.1), channel_id=1, replica_groups=mesh['ep'=16,'z'=16,'c'=2] {'z'}, dimensions={0} | all-to-all | bytes 131072 | tf_op jit(solution)/shard_map/all_to_all | solution.py:277
  73.5 0.7 total.1
Async XLA Ops:
  0.0 30.3 %collective-permute-start.1 = (bf16[2048,256]{1,0:T(8,128)(2,1)}, bf16[2048,256]{1,0:T(8,128)(2,1)}, u32[]{:S(2)}, u32[]{:S(2)}) collective-permute-start(bf16[2048,256]{1,0:T(8,128)(2,1)} %bitcast.14), channel_id=1, source_target_pairs={{0,1},{1,0},{2,3},{3,2},{4,5},{5,4},{6,7},{7,6},{8,9},{9,8},{10,11... | collective-permute-start | bytes 3145736 | tf_op jit(solution)/shard_map/ppermute | solution.py:234
  8.7 23.7 %collective-permute-start = (bf16[2048,256]{1,0:T(8,128)(2,1)}, bf16[2048,256]{1,0:T(8,128)(2,1)S(1)}, u32[]{:S(2)}, u32[]{:S(2)}) collective-permute-start(bf16[2048,256]{1,0:T(8,128)(2,1)} %bitcast.17), channel_id=1, source_target_pairs={{0,1},{1,0},{2,3},{3,2},{4,5},{5,4},{6,7},{7,6},{8,9},{9,8},{10,11... | collective-permute-start | bytes 3145736 | tf_op jit(solution)/shard_map/ppermute | solution.py:235
  10.7 21.8 %collective-permute-start.2 = (bf16[256,2048]{1,0:T(8,128)(2,1)}, bf16[256,2048]{1,0:T(8,128)(2,1)S(1)}, u32[]{:S(2)}, u32[]{:S(2)}) collective-permute-start(bf16[256,2048]{1,0:T(8,128)(2,1)} %bitcast.19), channel_id=1, source_target_pairs={{0,1},{1,0},{2,3},{3,2},{4,5},{5,4},{6,7},{7,6},{8,9},{9,8},{10,11... | collective-permute-start | bytes 3145736 | tf_op jit(solution)/shard_map/ppermute | solution.py:233
  15.4 14.9 %all-to-all-start = ((bf16[16,8,2048]{2,1,0:T(8,128)(2,1)}), bf16[16,8,2048]{2,1,0:T(8,128)(2,1)S(1)}, u32[]{:S(2)}, u32[]{:S(2)}) async-start(bf16[16,8,2048]{2,1,0:T(8,128)(2,1)} %bitcast.3), calls=%async_computation | async-start | bytes 1048576 | tf_op jit(solution)/shard_map/all_to_all | solution.py:230

commit v4 on v3

v4 whole, which is shorter than its diff:
```python
import jax
import jax.numpy as jnp
import numpy as np
from jax import lax
from jax.experimental import pallas as pl
from jax.experimental.pallas import tpu as pltpu
from jax.sharding import Mesh
from jax.sharding import PartitionSpec as P


WAY_IN = tuple(range(15, -1, -1))
WAY_BACK = tuple(range(31, -1, -1))
ALONG_Z = tuple((i + 10) % 16 for i in range(16))

LANES = 128
HALF = LANES // 2
F32 = jnp.float32
BF16 = jnp.bfloat16
SWAP = ((0, 1), (1, 0))


def params(mib):
    return pltpu.CompilerParams(vmem_limit_bytes=mib * 2**20)


def flipped(x):
    return pltpu.roll(x, HALF, axis=x.ndim - 1)


def column(row, eye):
    return jnp.sum(jnp.where(eye, row, 0), axis=1, keepdims=True)


def in_hbm(*arrays):
    return [pltpu.with_memory_space_constraint(x, pltpu.HBM) for x in arrays]


def started(sems, *pairs):
    copies = [pltpu.make_async_copy(src, dst, sems.at[i]) for i, (src, dst) in enumerate(pairs)]
    for copy in copies:
        copy.start()
    return copies


def slot_tables(each):
    spot = np.arange(each)
    back = np.array(WAY_BACK)
    tables = np.zeros((4, back.size * each), np.int32)
    mine = len(WAY_IN) * each
    tables[0, :mine] = np.repeat(WAY_IN, each)
    tables[1, :mine] = np.tile(spot, len(WAY_IN))
    tables[2] = np.repeat(back // 2, each)
    tables[3] = (back[:, None] % 2 * each + spot).reshape(-1)
    return tables


def dispatch_kernel(
    tok_hbm,
    picks_hbm,
    weight_hbm,
    tables_hbm,
    buffer_hbm,
    combine_ref,
    tok,
    picks,
    weight,
    tables,
    buffer,
    sems,
    out_sems,
):
    copies = started(
        sems, (tok_hbm, tok), (picks_hbm, picks), (weight_hbm, weight), (tables_hbm, tables)
    )
    rows, width = tok.shape
    mine = buffer.shape[0]
    each = rows // 4
    core = lax.axis_index("c")

    at_row = lax.broadcasted_iota(jnp.int32, (rows, rows), 0)
    at_col = lax.broadcasted_iota(jnp.int32, (rows, rows), 1)
    eye = at_row == at_col
    earlier = (at_col < at_row).astype(F32).astype(BF16)
    copies[1].wait()
    copies[2].wait()
    copies[3].wait()
    pick0 = column(picks[0:1, :], eye)
    pick1 = column(picks[1:2, :], eye)
    weight0 = column(weight[0:1, :], eye)
    weight1 = column(weight[1:2, :], eye)

    def placed(expert, place):
        is0 = pick0 == expert
        chosen = (is0 | (pick1 == expert)).astype(F32)
        rank = jnp.dot(earlier, chosen.astype(BF16), preferred_element_type=F32)
        return jnp.where(rank == place.astype(F32), chosen, 0.0), is0

    table, _ = placed(tables[0:1, :mine], tables[1:2, :mine] + core * each)
    spread = table.T.astype(BF16)
    copies[0].wait()
    chunks = out_sems.shape[0]
    leaving = []
    for i in range(chunks):
        at = pl.ds(i * (width // chunks), width // chunks)
        buffer[:, at] = jnp.dot(spread, tok[:, at], preferred_element_type=F32).astype(BF16)
        leaving.append(
            pltpu.make_async_copy(buffer.at[:, at], buffer_hbm.at[:, at], out_sems.at[i])
        )
        leaving[-1].start()
    table, is0 = placed(tables[2:3, :], tables[3:4, :])
    weights = table * jnp.where(is0, weight0, weight1)
    high = weights.astype(BF16)
    combine_ref[0:rows, :] = high
    combine_ref[rows:, :] = (weights - high.astype(F32)).astype(BF16)
    for copy in leaving:
        copy.wait()


def load_kernel(src_hbm, dst, sems):
    (copy,) = started(sems, (src_hbm.at[pl.ds(0, dst.shape[0]), :], dst))
    copy.wait()


def times(a, w):
    return jnp.dot(a, w[...], preferred_element_type=F32)


def hidden_of(gate, upper):
    return (gate / (1.0 + jnp.exp(-gate)) * upper).astype(BF16)


def hidden_kernel(
    received_ref,
    gain_ref,
    gate1,
    head0,
    gate0_hbm,
    up0_hbm,
    up1_hbm,
    down0_hbm,
    hidden_ref,
    down0_ref,
    rows_ref,
    tail0,
    up0,
    up1,
    sems,
):
    cut = head0.shape[0]
    units = up0.shape[1]
    copies = started(
        sems,
        (gate0_hbm.at[pl.ds(cut, tail0.shape[0]), :], tail0),
        (up0_hbm, up0),
        (up1_hbm, up1),
        (down0_hbm, down0_ref),
    )
    values = received_ref[...].astype(F32)
    scale = lax.rsqrt(jnp.mean(values * values, axis=-1, keepdims=True) + 1e-06)
    rows_ref[...] = (received_ref[...].astype(F32) * scale * gain_ref[...]).astype(BF16)
    gate = times(rows_ref[...], gate1)
    own = times(rows_ref[:, :cut], head0)
    copies[0].wait()
    own = own + times(rows_ref[:, cut:], tail0)
    copies[1].wait()
    hidden_ref[:, :units] = hidden_of(own, times(rows_ref[...], up0))
    copies[2].wait()
    hidden_ref[:, units:] = hidden_of(gate, times(rows_ref[...], up1))
    copies[3].wait()


def down_kernel(hidden_ref, down0_ref, down1_ref, out_ref):
    blocks, each, part = out_ref.shape
    rows, units = hidden_ref.shape[0], down0_ref.shape[0]
    low_lane = lax.broadcasted_iota(jnp.int32, (rows, LANES), 1) < HALF
    for m in range(part // LANES):
        pair = slice(2 * m * LANES, 2 * (m + 1) * LANES)
        out = times(hidden_ref[:, :units], down0_ref.at[:, pair])
        out = out + times(hidden_ref[:, units:], down1_ref.at[:, pair])
        a, b = out[:, :LANES], out[:, LANES:]
        low = jnp.where(low_lane, a, flipped(b))
        high = jnp.where(low_lane, flipped(a), b)
        for block in range(blocks):
            source, core = divmod(WAY_BACK[block], 2)
            first = WAY_IN.index(source) * each
            half = high if core else low
            out_ref[block, :, m * LANES : (m + 1) * LANES] = half[first : first + each].astype(BF16)


def combine_kernel(table_ref, back_ref, out_ref):
    rows = table_ref.shape[0] // 2
    half = rows // 2
    both = jnp.dot(table_ref[...], back_ref[...], preferred_element_type=F32)
    mixed = both[:rows] + both[rows:]
    low_lane = lax.broadcasted_iota(jnp.int32, (half, LANES), 1) < HALF
    for m in range(back_ref.shape[1] // LANES):
        at = slice(m * LANES, (m + 1) * LANES)
        a, b = mixed[:half, at], mixed[half:, at]
        out_ref[ALONG_Z.index(2 * m)] = jnp.where(low_lane, a, flipped(b)).astype(BF16)
        out_ref[ALONG_Z.index(2 * m + 1)] = jnp.where(low_lane, flipped(a), b).astype(BF16)


def total_kernel(parts_ref, out_ref):
    half = out_ref.shape[0] // 2
    total = jnp.sum(parts_ref[...].astype(F32), axis=0)
    out_ref[:half, :] = total[:, :HALF].astype(BF16)
    out_ref[half:, :] = flipped(total)[:, :HALF].astype(BF16)


def shape(dims, dtype):
    return jax.ShapeDtypeStruct(dims, dtype)


def shards(tokens, norm_gain, routes, gate_weights, expert_gate, expert_up, expert_down):
    rows, width = tokens.shape
    n_ep = lax.axis_size("ep")
    n_z = lax.axis_size("z")
    cap = rows // 2
    each = cap // 2
    slots = n_ep * cap
    mine = slots // 2
    part = width // 2
    w_gate, w_up, w_down = expert_gate[0], expert_up[0], expert_down[0]
    units = w_gate.shape[1]

    gain = norm_gain[None, :]
    picks = routes.T
    weights = gate_weights.T
    tables = jnp.asarray(slot_tables(each))
    hbm = pl.BlockSpec(memory_space=pltpu.HBM)
    vmem = pl.BlockSpec(memory_space=pltpu.VMEM)
    buffer, table = pl.pallas_call(
        dispatch_kernel,
        in_specs=[hbm] * 4,
        out_shape=(shape((mine, width), BF16), shape((2 * rows, slots), BF16)),
        out_specs=(hbm, vmem),
        scratch_shapes=[
            pltpu.VMEM(tokens.shape, tokens.dtype),
            pltpu.VMEM(picks.shape, picks.dtype),
            pltpu.VMEM(weights.shape, weights.dtype),
            pltpu.VMEM(tables.shape, tables.dtype),
            pltpu.VMEM((mine, width), BF16),
            pltpu.SemaphoreType.DMA((4,)),
            pltpu.SemaphoreType.DMA((4,)),
        ],
        compiler_params=params(8),
        name="dispatch",
    )(*in_hbm(tokens, picks, weights, tables))
    received = lax.all_to_all(
        buffer.reshape(n_ep, each, width), "ep", split_axis=0, concat_axis=0, tiled=True, axis_index_groups=[WAY_IN]
    ).reshape(mine, width)
    o_down = lax.ppermute(w_down, "c", SWAP)
    o_gate = lax.ppermute(w_gate, "c", SWAP)
    o_up = lax.ppermute(w_up, "c", SWAP)
    cut = width * 3 // 4
    head = pl.pallas_call(
        load_kernel,
        in_specs=[hbm],
        out_shape=shape((cut, units), BF16),
        scratch_shapes=[pltpu.SemaphoreType.DMA((1,))],
        compiler_params=params(8),
        name="load",
    )(*in_hbm(w_gate))
    hidden, down = pl.pallas_call(
        hidden_kernel,
        in_specs=[vmem] * 4 + [hbm] * 4,
        out_shape=(shape((mine, 2 * units), BF16), shape(w_down.shape, BF16)),
        scratch_shapes=[
            pltpu.VMEM((mine, width), BF16),
            pltpu.VMEM((width - cut, units), BF16),
            pltpu.VMEM(w_up.shape, BF16),
            pltpu.VMEM(w_up.shape, BF16),
            pltpu.SemaphoreType.DMA((4,)),
        ],
        compiler_params=params(8),
        name="hidden",
    )(received, gain, o_gate, head, *in_hbm(w_gate, w_up, o_up, w_down))
    outputs = pl.pallas_call(
        down_kernel,
        out_shape=shape((2 * n_ep, each, part), BF16),
        compiler_params=params(8),
        name="down",
    )(hidden, down, o_down)
    back = lax.all_to_all(
        outputs, ("ep", "c"), split_axis=0, concat_axis=0, tiled=True, axis_index_groups=[WAY_BACK]
    ).reshape(slots, part)
    packed = pl.pallas_call(
        combine_kernel,
        out_shape=shape((n_z, rows // 2, LANES), BF16),
        compiler_params=params(8),
        name="combine",
    )(table, back)
    parts = lax.all_to_all(packed, "z", split_axis=0, concat_axis=0, tiled=True, axis_index_groups=[ALONG_Z])
    return pl.pallas_call(
        total_kernel,
        out_shape=shape((rows, HALF), BF16),
        compiler_params=params(8),
        name="total",
    )(parts)


def solution(mesh):
    n_ep, n_tp = mesh.devices.shape
    chips = Mesh(np.asarray(mesh.devices).reshape(n_ep, n_tp // 2, 2), ("ep", "z", "c"))
    tp = ("z", "c")
    placed = (
        P("ep", None),
        P(),
        P("ep", None),
        P("ep", None),
        P("ep", None, tp),
        P("ep", None, tp),
        P("ep", tp, None),
    )
    return jax.shard_map(
        shards, mesh=chips, in_specs=placed, out_specs=P("ep", tp), check_vma=False
    )
```

time: 74.6 us -> 67.1 us (0.90)
  blocking collectives: 39.7 us -> 34 us
  waiting for transfers between devices: 10.2 us -> 6.38 us
  starting transfers between devices: 16.7 us -> 19.2 us
    all_to_all x2, blocking collectives: 39.7 us -> 34 us  [the longest x1 18.3 us: shards(): lax.all_to_all(packed, 'z', split_axis=0, concat_axis=0, tiled=True, axis...]
    all_to_all x1, waiting for transfers between devices: 10.1 us -> 6.38 us  [shards(): lax.all_to_all(buffer.reshape(n_ep, each, width), 'ep', split_axis=0, con...]
    all_to_all x1, starting transfers between devices: 3.58 us -> 6.09 us  [shards(): lax.all_to_all(buffer.reshape(n_ep, each, width), 'ep', split_axis=0, con...]
where the time goes in v4:
time: 67.1 us; the launch traced here: 66.7 us
  blocking collectives  34 us (51%)
  starting transfers between devices  19.2 us (29%)
  Pallas kernels  7.07 us (11%)
  waiting for transfers between devices  6.38 us (10%)
    all_to_all x1, blocking collectives, shards(): lax.all_to_all(packed, 'z', split_axis=0, concat_axis=0, tiled=True, axis...  18.3 us
    all_to_all x1, blocking collectives, shards(): lax.all_to_all(outputs, ('ep', 'c'), split_axis=0, concat_axis=0, tiled=T...  15.8 us
    ppermute x1, starting transfers between devices, shards(): o_gate = lax.ppermute(w_gate, 'c', SWAP)  8.74 us
    all_to_all x1, waiting for transfers between devices, shards(): lax.all_to_all(buffer.reshape(n_ep, each, width), 'ep', split_axis=0, con...  6.38 us
    all_to_all x1, starting transfers between devices, shards(): lax.all_to_all(buffer.reshape(n_ep, each, width), 'ep', split_axis=0, con...  6.09 us
    ppermute x1, starting transfers between devices, shards(): o_down = lax.ppermute(w_down, 'c', SWAP)  2.41 us
    pallas_call x1, Pallas kernels, shards(): pl.pallas_call(hidden_kernel, in_specs=[vmem] * 4 + [hbm] * 4, out_shape=...  2.26 us
    pallas_call x1, Pallas kernels, shards(): pl.pallas_call(dispatch_kernel, in_specs=[hbm] * 4, out_shape=(shape((min...  2.16 us
  transfers between devices with their start and end apart: 4, of which 1 were waited for; matrix products, arithmetic and copies ran while one was open for 0% of the time, Pallas kernels for 8%

profile of v4, /device:TPU:1, one launch (start us, length us, event | category | flops | bytes accessed | tf_op | source)
XLA Modules:
  0.0 66.7 jit_solution(11369957131307781906)
XLA Ops:
  0.0 8.7 %collective-permute-start = (bf16[2048,256]{1,0:T(8,128)(2,1)}, bf16[2048,256]{1,0:T(8,128)(2,1)S(1)}, u32[]{:S(2)}, u32[]{:S(2)}) collective-permute-start(bf16[2048,256]{1,0:T(8,128)(2,1)} %bitcast.12), channel_id=1, source_target_pairs={{0,1},{1,0},{2,3},{3,2},{4,5},{5,4},{6,7},{7,6},{8,9},{9,8},{10,11... | collective-permute-start | bytes 3145736 | tf_op jit(solution)/shard_map/ppermute | solution.py:253
  8.7 1.9 %collective-permute-start.1 = (bf16[2048,256]{1,0:T(8,128)(2,1)}, bf16[2048,256]{1,0:T(8,128)(2,1)}, u32[]{:S(2)}, u32[]{:S(2)}) collective-permute-start(bf16[2048,256]{1,0:T(8,128)(2,1)} %bitcast.15), channel_id=1, source_target_pairs={{0,1},{1,0},{2,3},{3,2},{4,5},{5,4},{6,7},{7,6},{8,9},{9,8},{10,11... | collective-permute-start | bytes 3145736 | tf_op jit(solution)/shard_map/ppermute | solution.py:254
  10.7 2.4 %collective-permute-start.2 = (bf16[256,2048]{1,0:T(8,128)(2,1)}, bf16[256,2048]{1,0:T(8,128)(2,1)S(1)}, u32[]{:S(2)}, u32[]{:S(2)}) collective-permute-start(bf16[256,2048]{1,0:T(8,128)(2,1)} %bitcast.17), channel_id=1, source_target_pairs={{0,1},{1,0},{2,3},{3,2},{4,5},{5,4},{6,7},{7,6},{8,9},{9,8},{10,11... | collective-permute-start | bytes 3145736 | tf_op jit(solution)/shard_map/ppermute | solution.py:252
  13.1 2.2 %dispatch.1 = (bf16[128,2048]{1,0:T(8,128)(2,1)}, bf16[64,256]{1,0:T(8,128)(2,1)S(1)}) custom-call(bf16[32,2048]{1,0:T(8,128)(2,1)} %tok_hbm.1, s32[2,32]{1,0:T(2,128)} %bitcast.19, f32[2,32]{1,0:T(2,128)} %bitcast.20, s32[4,256]{1,0:T(4,128)} %constant.2.clone.tables_hbm), custom_call_target="tpu_custom_call" | custom-call | tf_op jit(solution)/shard_map/dispatch/pallas_call | solution.py:232
  15.3 6.1 %all-to-all-start = ((bf16[16,8,2048]{2,1,0:T(8,128)(2,1)}), bf16[16,8,2048]{2,1,0:T(8,128)(2,1)S(1)}, u32[]{:S(2)}, u32[]{:S(2)}) async-start(bf16[16,8,2048]{2,1,0:T(8,128)(2,1)} %bitcast.2), calls=%async_computation | async-start | bytes 1048576 | tf_op jit(solution)/shard_map/all_to_all | solution.py:249
  21.4 0.0 copy-start
  21.4 1.1 %load.1.head0 = bf16[1536,256]{1,0:T(8,128)(2,1)S(1)} custom-call(bf16[2048,256]{1,0:T(8,128)(2,1)} %bitcast.13), custom_call_target="tpu_custom_call" | custom-call | tf_op jit(solution)/shard_map/load/pallas_call | solution.py:256
  22.5 6.4 %all-to-all-done = bf16[16,8,2048]{2,1,0:T(8,128)(2,1)S(1)} async-done(((bf16[16,8,2048]{2,1,0:T(8,128)(2,1)}), bf16[16,8,2048]{2,1,0:T(8,128)(2,1)S(1)}, u32[]{:S(2)}, u32[]{:S(2)}) %all-to-all-start) | async-done | bytes 524320 | tf_op jit(solution)/shard_map/all_to_all | solution.py:249
  28.9 0.0 collective-permute-done.gate1
  28.9 0.0 collective-permute-done.1.up1_hbm
  28.9 0.0 copy-done
  28.9 2.3 %hidden.1 = (bf16[128,512]{1,0:T(8,128)(2,1)S(1)}, bf16[256,2048]{1,0:T(8,128)(2,1)S(1)}) custom-call(bf16[128,2048]{1,0:T(8,128)(2,1)S(1)} %bitcast.9, f32[1,2048]{1,0:T(1,128)S(1)} %bitcast.11, bf16[2048,256]{1,0:T(8,128)(2,1)S(1)} %collective-permute-done.gate1, bf16[1536,256]{1,0:T(8,128)(2,1)S(1)} %load.1.head0, bf16[2048,256]{1,0:T(8,128)(2,1)} %bitcast.14, ...), custom_call_target="tpu_custom_call" | custom-call | tf_op jit(solution)/shard_map/hidden/pallas_call | solution.py:264
  31.2 0.0 collective-permute-done.2.down1_ref
  31.2 0.5 down.1
  31.7 15.8 %all_to_all.15 = bf16[32,8,1024]{2,1,0:T(8,128)(2,1)S(1)} all-to-all(bf16[32,8,1024]{2,1,0:T(8,128)(2,1)S(1)} %down.1), channel_id=1, replica_groups={{481,480,449,448,417,416,385,384,353,352,321,320,289,288,257,256,225,22..., dimensions={0} | all-to-all | bytes 1048576 | tf_op jit(solution)/shard_map/all_to_all | solution.py:284
  47.5 0.3 combine.1
  47.8 18.3 %all_to_all.16.parts_ref = bf16[16,16,128]{2,1,0:T(8,128)(2,1)S(1)} all-to-all(bf16[16,16,128]{2,1,0:T(8,128)(2,1)S(1)} %combine.1), channel_id=1, replica_groups={{20,22,24,26,28,30,0,2,4,6,8,10,12,14,16,18},{21,23,25,27,29,31,1,3,5,7..., dimensions={0} | all-to-all | bytes 131072 | tf_op jit(solution)/shard_map/all_to_all | solution.py:293
  66.1 0.7 %total.1 = bf16[32,64]{1,0:T(8,128)(2,1)} custom-call(bf16[16,16,128]{2,1,0:T(8,128)(2,1)S(1)} %all_to_all.16.parts_ref), custom_call_target="tpu_custom_call" | custom-call | tf_op jit(solution)/shard_map/total/pallas_call | solution.py:294
Async XLA Ops:
  0.0 28.9 %collective-permute-start = (bf16[2048,256]{1,0:T(8,128)(2,1)}, bf16[2048,256]{1,0:T(8,128)(2,1)S(1)}, u32[]{:S(2)}, u32[]{:S(2)}) collective-permute-start(bf16[2048,256]{1,0:T(8,128)(2,1)} %bitcast.12), channel_id=1, source_target_pairs={{0,1},{1,0},{2,3},{3,2},{4,5},{5,4},{6,7},{7,6},{8,9},{9,8},{10,11... | collective-permute-start | bytes 3145736 | tf_op jit(solution)/shard_map/ppermute | solution.py:253
  8.7 20.2 %collective-permute-start.1 = (bf16[2048,256]{1,0:T(8,128)(2,1)}, bf16[2048,256]{1,0:T(8,128)(2,1)}, u32[]{:S(2)}, u32[]{:S(2)}) collective-permute-start(bf16[2048,256]{1,0:T(8,128)(2,1)} %bitcast.15), channel_id=1, source_target_pairs={{0,1},{1,0},{2,3},{3,2},{4,5},{5,4},{6,7},{7,6},{8,9},{9,8},{10,11... | collective-permute-start | bytes 3145736 | tf_op jit(solution)/shard_map/ppermute | solution.py:254
  10.7 20.5 %collective-permute-start.2 = (bf16[256,2048]{1,0:T(8,128)(2,1)}, bf16[256,2048]{1,0:T(8,128)(2,1)S(1)}, u32[]{:S(2)}, u32[]{:S(2)}) collective-permute-start(bf16[256,2048]{1,0:T(8,128)(2,1)} %bitcast.17), channel_id=1, source_target_pairs={{0,1},{1,0},{2,3},{3,2},{4,5},{5,4},{6,7},{7,6},{8,9},{9,8},{10,11... | collective-permute-start | bytes 3145736 | tf_op jit(solution)/shard_map/ppermute | solution.py:252
  15.3 13.6 %all-to-all-start = ((bf16[16,8,2048]{2,1,0:T(8,128)(2,1)}), bf16[16,8,2048]{2,1,0:T(8,128)(2,1)S(1)}, u32[]{:S(2)}, u32[]{:S(2)}) async-start(bf16[16,8,2048]{2,1,0:T(8,128)(2,1)} %bitcast.2), calls=%async_computation | async-start | bytes 1048576 | tf_op jit(solution)/shard_map/all_to_all | solution.py:249
  21.4 7.5 %copy-start = (f32[2048]{0:T(1024)S(1)}, f32[2048]{0:T(1024)}, u32[]{:S(2)}) copy-start(f32[2048]{0:T(1024)} %param.9) | copy-start | bytes 24580

commit v5 on v4

--- a/solution.py
+++ b/solution.py
@@ -8,9 +8,20 @@
 from jax.sharding import PartitionSpec as P
 
 
+SIDE = 4
+
+
+def hops(chip):
+    y, x = divmod(chip, SIDE)
+    return min(y, SIDE - y) + min(x, SIDE - x)
+
+
 WAY_IN = tuple(range(15, -1, -1))
-WAY_BACK = tuple(range(31, -1, -1))
+WAY_BACK = tuple(
+    2 * chip + core for chip in sorted(range(16), key=lambda e: (-hops(e), e)) for core in (1, 0)
+)
 ALONG_Z = tuple((i + 10) % 16 for i in range(16))
+
 
 LANES = 128
 HALF = LANES // 2
@@ -43,15 +54,9 @@
 
 
 def slot_tables(each):
-    spot = np.arange(each)
-    back = np.array(WAY_BACK)
-    tables = np.zeros((4, back.size * each), np.int32)
-    mine = len(WAY_IN) * each
-    tables[0, :mine] = np.repeat(WAY_IN, each)
-    tables[1, :mine] = np.tile(spot, len(WAY_IN))
-    tables[2] = np.repeat(back // 2, each)
-    tables[3] = (back[:, None] % 2 * each + spot).reshape(-1)
-    return tables
+    chip, core = np.divmod(np.array(WAY_BACK), 2)
+    rank = core[:, None] * each + np.arange(each)
+    return np.stack([np.repeat(chip, each), rank.reshape(-1)]).astype(np.int32)
 
 
 def dispatch_kernel(
@@ -75,28 +80,19 @@
     rows, width = tok.shape
     mine = buffer.shape[0]
     each = rows // 4
-    core = lax.axis_index("c")
+    half = lax.axis_index("c")
 
     at_row = lax.broadcasted_iota(jnp.int32, (rows, rows), 0)
     at_col = lax.broadcasted_iota(jnp.int32, (rows, rows), 1)
     eye = at_row == at_col
-    earlier = (at_col < at_row).astype(F32).astype(BF16)
+    before = (at_row < at_col).astype(F32).astype(BF16)
+    slot = lax.broadcasted_iota(jnp.int32, (mine, rows), 0)
+    expert = len(WAY_IN) - 1 - slot // each
+    place = (slot % each + half * each).astype(F32)
     copies[1].wait()
-    copies[2].wait()
-    copies[3].wait()
-    pick0 = column(picks[0:1, :], eye)
-    pick1 = column(picks[1:2, :], eye)
-    weight0 = column(weight[0:1, :], eye)
-    weight1 = column(weight[1:2, :], eye)
-
-    def placed(expert, place):
-        is0 = pick0 == expert
-        chosen = (is0 | (pick1 == expert)).astype(F32)
-        rank = jnp.dot(earlier, chosen.astype(BF16), preferred_element_type=F32)
-        return jnp.where(rank == place.astype(F32), chosen, 0.0), is0
-
-    table, _ = placed(tables[0:1, :mine], tables[1:2, :mine] + core * each)
-    spread = table.T.astype(BF16)
+    chosen = ((picks[0:1, :] == expert) | (picks[1:2, :] == expert)).astype(F32)
+    rank = jnp.dot(chosen.astype(BF16), before, preferred_element_type=F32)
+    spread = jnp.where(rank == place, chosen, 0.0).astype(BF16)
     copies[0].wait()
     chunks = out_sems.shape[0]
     leaving = []
@@ -107,7 +103,17 @@
             pltpu.make_async_copy(buffer.at[:, at], buffer_hbm.at[:, at], out_sems.at[i])
         )
         leaving[-1].start()
-    table, is0 = placed(tables[2:3, :], tables[3:4, :])
+    copies[2].wait()
+    copies[3].wait()
+    pick0 = column(picks[0:1, :], eye)
+    pick1 = column(picks[1:2, :], eye)
+    weight0 = column(weight[0:1, :], eye)
+    weight1 = column(weight[1:2, :], eye)
+    earlier = (at_col < at_row).astype(F32).astype(BF16)
+    is0 = pick0 == tables[0:1, :]
+    chosen = (is0 | (pick1 == tables[0:1, :])).astype(F32)
+    rank = jnp.dot(earlier, chosen.astype(BF16), preferred_element_type=F32)
+    table = jnp.where(rank == tables[1:2, :].astype(F32), chosen, 0.0)
     weights = table * jnp.where(is0, weight0, weight1)
     high = weights.astype(BF16)
     combine_ref[0:rows, :] = high
@@ -247,7 +253,12 @@
         name="dispatch",
     )(*in_hbm(tokens, picks, weights, tables))
     received = lax.all_to_all(
-        buffer.reshape(n_ep, each, width), "ep", split_axis=0, concat_axis=0, tiled=True, axis_index_groups=[WAY_IN]
+        buffer.reshape(n_ep, each, width),
+        "ep",
+        split_axis=0,
+        concat_axis=0,
+        tiled=True,
+        axis_index_groups=[WAY_IN],
     ).reshape(mine, width)
     o_down = lax.ppermute(w_down, "c", SWAP)
     o_gate = lax.ppermute(w_gate, "c", SWAP)

time: 67.1 us -> 66.4 us (0.990)
  blocking collectives: 34 us -> 33.3 us
where the time goes in v5:
time: 66.4 us; the launch traced here: 65.8 us
  blocking collectives  33.3 us (50%)
  starting transfers between devices  19.2 us (29%)
  Pallas kernels  6.88 us (10%)
  waiting for transfers between devices  6.38 us (10%)
    all_to_all x1, blocking collectives, shards(): lax.all_to_all(packed, 'z', split_axis=0, concat_axis=0, tiled=True, axis...  18.1 us
    all_to_all x1, blocking collectives, shards(): lax.all_to_all(outputs, ('ep', 'c'), split_axis=0, concat_axis=0, tiled=T...  15.2 us
    ppermute x1, starting transfers between devices, shards(): o_gate = lax.ppermute(w_gate, 'c', SWAP)  8.74 us
    all_to_all x1, waiting for transfers between devices, shards(): lax.all_to_all(buffer.reshape(n_ep, each, width), 'ep', split_axis=0, con...  6.38 us
    all_to_all x1, starting transfers between devices, shards(): lax.all_to_all(buffer.reshape(n_ep, each, width), 'ep', split_axis=0, con...  6.09 us
    ppermute x1, starting transfers between devices, shards(): o_down = lax.ppermute(w_down, 'c', SWAP)  2.41 us
    pallas_call x1, Pallas kernels, shards(): pl.pallas_call(hidden_kernel, in_specs=[vmem] * 4 + [hbm] * 4, out_shape=...  2.26 us
    pallas_call x1, Pallas kernels, shards(): pl.pallas_call(dispatch_kernel, in_specs=[hbm] * 4, out_shape=(shape((min...  1.97 us
  transfers between devices with their start and end apart: 4, of which 1 were waited for; matrix products, arithmetic and copies ran while one was open for 0% of the time, Pallas kernels for 8%

profile of v5, /device:TPU:1, one launch (start us, length us, event | category | flops | bytes accessed | tf_op | source)
XLA Modules:
  0.0 65.8 jit_solution(13653433325060892737)
XLA Ops:
  0.0 8.7 %collective-permute-start = (bf16[2048,256]{1,0:T(8,128)(2,1)}, bf16[2048,256]{1,0:T(8,128)(2,1)S(1)}, u32[]{:S(2)}, u32[]{:S(2)}) collective-permute-start(bf16[2048,256]{1,0:T(8,128)(2,1)} %bitcast.12), channel_id=1, source_target_pairs={{0,1},{1,0},{2,3},{3,2},{4,5},{5,4},{6,7},{7,6},{8,9},{9,8},{10,11... | collective-permute-start | bytes 3145736 | tf_op jit(solution)/shard_map/ppermute | solution.py:264
  8.7 1.9 %collective-permute-start.1 = (bf16[2048,256]{1,0:T(8,128)(2,1)}, bf16[2048,256]{1,0:T(8,128)(2,1)}, u32[]{:S(2)}, u32[]{:S(2)}) collective-permute-start(bf16[2048,256]{1,0:T(8,128)(2,1)} %bitcast.15), channel_id=1, source_target_pairs={{0,1},{1,0},{2,3},{3,2},{4,5},{5,4},{6,7},{7,6},{8,9},{9,8},{10,11... | collective-permute-start | bytes 3145736 | tf_op jit(solution)/shard_map/ppermute | solution.py:265
  10.7 2.4 %collective-permute-start.2 = (bf16[256,2048]{1,0:T(8,128)(2,1)}, bf16[256,2048]{1,0:T(8,128)(2,1)S(1)}, u32[]{:S(2)}, u32[]{:S(2)}) collective-permute-start(bf16[256,2048]{1,0:T(8,128)(2,1)} %bitcast.17), channel_id=1, source_target_pairs={{0,1},{1,0},{2,3},{3,2},{4,5},{5,4},{6,7},{7,6},{8,9},{9,8},{10,11... | collective-permute-start | bytes 3145736 | tf_op jit(solution)/shard_map/ppermute | solution.py:263
  13.1 2.0 %dispatch.1 = (bf16[128,2048]{1,0:T(8,128)(2,1)}, bf16[64,256]{1,0:T(8,128)(2,1)S(1)}) custom-call(bf16[32,2048]{1,0:T(8,128)(2,1)} %tok_hbm.1, s32[2,32]{1,0:T(2,128)} %bitcast.19, f32[2,32]{1,0:T(2,128)} %bitcast.20, s32[2,256]{1,0:T(2,128)} %constant.2.clone.tables_hbm), custom_call_target="tpu_custom_call" | custom-call | tf_op jit(solution)/shard_map/dispatch/pallas_call | solution.py:238
  15.1 6.1 %all-to-all-start = ((bf16[16,8,2048]{2,1,0:T(8,128)(2,1)}), bf16[16,8,2048]{2,1,0:T(8,128)(2,1)S(1)}, u32[]{:S(2)}, u32[]{:S(2)}) async-start(bf16[16,8,2048]{2,1,0:T(8,128)(2,1)} %bitcast.2), calls=%async_computation | async-start | bytes 1048576 | tf_op jit(solution)/shard_map/all_to_all | solution.py:255
  21.2 0.0 copy-start
  21.2 1.1 %load.1.head0 = bf16[1536,256]{1,0:T(8,128)(2,1)S(1)} custom-call(bf16[2048,256]{1,0:T(8,128)(2,1)} %bitcast.13), custom_call_target="tpu_custom_call" | custom-call | tf_op jit(solution)/shard_map/load/pallas_call | solution.py:267
  22.3 6.4 %all-to-all-done = bf16[16,8,2048]{2,1,0:T(8,128)(2,1)S(1)} async-done(((bf16[16,8,2048]{2,1,0:T(8,128)(2,1)}), bf16[16,8,2048]{2,1,0:T(8,128)(2,1)S(1)}, u32[]{:S(2)}, u32[]{:S(2)}) %all-to-all-start) | async-done | bytes 524320 | tf_op jit(solution)/shard_map/all_to_all | solution.py:255
  28.7 0.0 collective-permute-done.gate1
  28.7 0.0 collective-permute-done.1.up1_hbm
  28.7 0.0 copy-done
  28.7 2.3 %hidden.1 = (bf16[128,512]{1,0:T(8,128)(2,1)S(1)}, bf16[256,2048]{1,0:T(8,128)(2,1)S(1)}) custom-call(bf16[128,2048]{1,0:T(8,128)(2,1)S(1)} %bitcast.9, f32[1,2048]{1,0:T(1,128)S(1)} %bitcast.11, bf16[2048,256]{1,0:T(8,128)(2,1)S(1)} %collective-permute-done.gate1, bf16[1536,256]{1,0:T(8,128)(2,1)S(1)} %load.1.head0, bf16[2048,256]{1,0:T(8,128)(2,1)} %bitcast.14, ...), custom_call_target="tpu_custom_call" | custom-call | tf_op jit(solution)/shard_map/hidden/pallas_call | solution.py:275
  31.0 0.0 collective-permute-done.2.down1_ref
  31.0 0.5 down.1
  31.5 15.2 %all_to_all.15 = bf16[32,8,1024]{2,1,0:T(8,128)(2,1)S(1)} all-to-all(bf16[32,8,1024]{2,1,0:T(8,128)(2,1)S(1)} %down.1), channel_id=1, replica_groups={{321,320,193,192,289,288,353,352,449,448,65,64,161,160,225,224,257,256,..., dimensions={0} | all-to-all | bytes 1048576 | tf_op jit(solution)/shard_map/all_to_all | solution.py:295
  46.7 0.3 combine.1
  47.0 18.1 %all_to_all.16.parts_ref = bf16[16,16,128]{2,1,0:T(8,128)(2,1)S(1)} all-to-all(bf16[16,16,128]{2,1,0:T(8,128)(2,1)S(1)} %combine.1), channel_id=1, replica_groups={{20,22,24,26,28,30,0,2,4,6,8,10,12,14,16,18},{21,23,25,27,29,31,1,3,5,7..., dimensions={0} | all-to-all | bytes 131072 | tf_op jit(solution)/shard_map/all_to_all | solution.py:304
  65.1 0.7 %total.1 = bf16[32,64]{1,0:T(8,128)(2,1)} custom-call(bf16[16,16,128]{2,1,0:T(8,128)(2,1)S(1)} %all_to_all.16.parts_ref), custom_call_target="tpu_custom_call" | custom-call | tf_op jit(solution)/shard_map/total/pallas_call | solution.py:305
Async XLA Ops:
  0.0 28.7 %collective-permute-start = (bf16[2048,256]{1,0:T(8,128)(2,1)}, bf16[2048,256]{1,0:T(8,128)(2,1)S(1)}, u32[]{:S(2)}, u32[]{:S(2)}) collective-permute-start(bf16[2048,256]{1,0:T(8,128)(2,1)} %bitcast.12), channel_id=1, source_target_pairs={{0,1},{1,0},{2,3},{3,2},{4,5},{5,4},{6,7},{7,6},{8,9},{9,8},{10,11... | collective-permute-start | bytes 3145736 | tf_op jit(solution)/shard_map/ppermute | solution.py:264
  8.7 20.0 %collective-permute-start.1 = (bf16[2048,256]{1,0:T(8,128)(2,1)}, bf16[2048,256]{1,0:T(8,128)(2,1)}, u32[]{:S(2)}, u32[]{:S(2)}) collective-permute-start(bf16[2048,256]{1,0:T(8,128)(2,1)} %bitcast.15), channel_id=1, source_target_pairs={{0,1},{1,0},{2,3},{3,2},{4,5},{5,4},{6,7},{7,6},{8,9},{9,8},{10,11... | collective-permute-start | bytes 3145736 | tf_op jit(solution)/shard_map/ppermute | solution.py:265
  10.7 20.3 %collective-permute-start.2 = (bf16[256,2048]{1,0:T(8,128)(2,1)}, bf16[256,2048]{1,0:T(8,128)(2,1)S(1)}, u32[]{:S(2)}, u32[]{:S(2)}) collective-permute-start(bf16[256,2048]{1,0:T(8,128)(2,1)} %bitcast.17), channel_id=1, source_target_pairs={{0,1},{1,0},{2,3},{3,2},{4,5},{5,4},{6,7},{7,6},{8,9},{9,8},{10,11... | collective-permute-start | bytes 3145736 | tf_op jit(solution)/shard_map/ppermute | solution.py:263
  15.1 13.6 %all-to-all-start = ((bf16[16,8,2048]{2,1,0:T(8,128)(2,1)}), bf16[16,8,2048]{2,1,0:T(8,128)(2,1)S(1)}, u32[]{:S(2)}, u32[]{:S(2)}) async-start(bf16[16,8,2048]{2,1,0:T(8,128)(2,1)} %bitcast.2), calls=%async_computation | async-start | bytes 1048576 | tf_op jit(solution)/shard_map/all_to_all | solution.py:255
  21.2 7.5 %copy-start = (f32[2048]{0:T(1024)S(1)}, f32[2048]{0:T(1024)}, u32[]{:S(2)}) copy-start(f32[2048]{0:T(1024)} %param.9) | copy-start | bytes 24580

commit v6 on v5

--- a/solution.py
+++ b/solution.py
@@ -16,7 +16,7 @@
     return min(y, SIDE - y) + min(x, SIDE - x)
 
 
-WAY_IN = tuple(range(15, -1, -1))
+WAY_IN = tuple(sorted(range(16), key=lambda e: (-hops(e), -e)))
 WAY_BACK = tuple(
     2 * chip + core for chip in sorted(range(16), key=lambda e: (-hops(e), e)) for core in (1, 0)
 )
@@ -87,7 +87,9 @@
     eye = at_row == at_col
     before = (at_row < at_col).astype(F32).astype(BF16)
     slot = lax.broadcasted_iota(jnp.int32, (mine, rows), 0)
-    expert = len(WAY_IN) - 1 - slot // each
+    expert = jnp.zeros_like(slot)
+    for block, chip in enumerate(WAY_IN):
+        expert = jnp.where(slot // each == block, chip, expert)
     place = (slot % each + half * each).astype(F32)
     copies[1].wait()
     chosen = ((picks[0:1, :] == expert) | (picks[1:2, :] == expert)).astype(F32)

time: 66.4 us -> 65.9 us (level)
  waiting for transfers between devices: 6.38 us -> 5.64 us
    all_to_all x1, waiting for transfers between devices: 6.38 us -> 5.63 us  [shards(): lax.all_to_all(buffer.reshape(n_ep, each, width), 'ep', split_axis=0, con...]
where the time goes in v6:
time: 65.9 us; the launch traced here: 65.3 us
  blocking collectives  32.9 us (50%)
  starting transfers between devices  19.7 us (30%)
  Pallas kernels  6.88 us (10%)
  waiting for transfers between devices  5.64 us (9%)
    all_to_all x1, blocking collectives, shards(): lax.all_to_all(packed, 'z', split_axis=0, concat_axis=0, tiled=True, axis...  17.9 us
    all_to_all x1, blocking collectives, shards(): lax.all_to_all(outputs, ('ep', 'c'), split_axis=0, concat_axis=0, tiled=T...  15 us
    ppermute x1, starting transfers between devices, shards(): o_gate = lax.ppermute(w_gate, 'c', SWAP)  8.74 us
    all_to_all x1, starting transfers between devices, shards(): lax.all_to_all(buffer.reshape(n_ep, each, width), 'ep', split_axis=0, con...  6.68 us
    all_to_all x1, waiting for transfers between devices, shards(): lax.all_to_all(buffer.reshape(n_ep, each, width), 'ep', split_axis=0, con...  5.63 us
    ppermute x1, starting transfers between devices, shards(): o_down = lax.ppermute(w_down, 'c', SWAP)  2.41 us
    pallas_call x1, Pallas kernels, shards(): pl.pallas_call(hidden_kernel, in_specs=[vmem] * 4 + [hbm] * 4, out_shape=...  2.25 us
    pallas_call x1, Pallas kernels, shards(): pl.pallas_call(dispatch_kernel, in_specs=[hbm] * 4, out_shape=(shape((min...  1.97 us
  transfers between devices with their start and end apart: 4, of which 1 were waited for; matrix products, arithmetic and copies ran while one was open for 0% of the time, Pallas kernels for 8%

profile of v6, /device:TPU:1, one launch (start us, length us, event | category | flops | bytes accessed | tf_op | source)
XLA Modules:
  0.0 65.3 jit_solution(2726881942377474399)
XLA Ops:
  0.0 8.7 %collective-permute-start = (bf16[2048,256]{1,0:T(8,128)(2,1)}, bf16[2048,256]{1,0:T(8,128)(2,1)S(1)}, u32[]{:S(2)}, u32[]{:S(2)}) collective-permute-start(bf16[2048,256]{1,0:T(8,128)(2,1)} %bitcast.12), channel_id=1, source_target_pairs={{0,1},{1,0},{2,3},{3,2},{4,5},{5,4},{6,7},{7,6},{8,9},{9,8},{10,11... | collective-permute-start | bytes 3145736 | tf_op jit(solution)/shard_map/ppermute | solution.py:266
  8.7 1.9 %collective-permute-start.1 = (bf16[2048,256]{1,0:T(8,128)(2,1)}, bf16[2048,256]{1,0:T(8,128)(2,1)}, u32[]{:S(2)}, u32[]{:S(2)}) collective-permute-start(bf16[2048,256]{1,0:T(8,128)(2,1)} %bitcast.15), channel_id=1, source_target_pairs={{0,1},{1,0},{2,3},{3,2},{4,5},{5,4},{6,7},{7,6},{8,9},{9,8},{10,11... | collective-permute-start | bytes 3145736 | tf_op jit(solution)/shard_map/ppermute | solution.py:267
  10.7 2.4 %collective-permute-start.2 = (bf16[256,2048]{1,0:T(8,128)(2,1)}, bf16[256,2048]{1,0:T(8,128)(2,1)S(1)}, u32[]{:S(2)}, u32[]{:S(2)}) collective-permute-start(bf16[256,2048]{1,0:T(8,128)(2,1)} %bitcast.17), channel_id=1, source_target_pairs={{0,1},{1,0},{2,3},{3,2},{4,5},{5,4},{6,7},{7,6},{8,9},{9,8},{10,11... | collective-permute-start | bytes 3145736 | tf_op jit(solution)/shard_map/ppermute | solution.py:265
  13.1 2.0 %dispatch.1 = (bf16[128,2048]{1,0:T(8,128)(2,1)}, bf16[64,256]{1,0:T(8,128)(2,1)S(1)}) custom-call(bf16[32,2048]{1,0:T(8,128)(2,1)} %tok_hbm.1, s32[2,32]{1,0:T(2,128)} %bitcast.19, f32[2,32]{1,0:T(2,128)} %bitcast.20, s32[2,256]{1,0:T(2,128)} %constant.2.clone.tables_hbm), custom_call_target="tpu_custom_call" | custom-call | tf_op jit(solution)/shard_map/dispatch/pallas_call | solution.py:240
  15.1 6.7 %all-to-all-start = ((bf16[16,8,2048]{2,1,0:T(8,128)(2,1)}), bf16[16,8,2048]{2,1,0:T(8,128)(2,1)S(1)}, u32[]{:S(2)}, u32[]{:S(2)}) async-start(bf16[16,8,2048]{2,1,0:T(8,128)(2,1)} %bitcast.2), calls=%async_computation | async-start | bytes 1048576 | tf_op jit(solution)/shard_map/all_to_all | solution.py:257
  21.7 0.0 copy-start
  21.8 1.1 %load.1.head0 = bf16[1536,256]{1,0:T(8,128)(2,1)S(1)} custom-call(bf16[2048,256]{1,0:T(8,128)(2,1)} %bitcast.13), custom_call_target="tpu_custom_call" | custom-call | tf_op jit(solution)/shard_map/load/pallas_call | solution.py:269
  22.9 5.6 %all-to-all-done = bf16[16,8,2048]{2,1,0:T(8,128)(2,1)S(1)} async-done(((bf16[16,8,2048]{2,1,0:T(8,128)(2,1)}), bf16[16,8,2048]{2,1,0:T(8,128)(2,1)S(1)}, u32[]{:S(2)}, u32[]{:S(2)}) %all-to-all-start) | async-done | bytes 524320 | tf_op jit(solution)/shard_map/all_to_all | solution.py:257
  28.5 0.0 collective-permute-done.gate1
  28.5 0.0 collective-permute-done.1.up1_hbm
  28.6 0.0 copy-done
  28.6 2.3 %hidden.1 = (bf16[128,512]{1,0:T(8,128)(2,1)S(1)}, bf16[256,2048]{1,0:T(8,128)(2,1)S(1)}) custom-call(bf16[128,2048]{1,0:T(8,128)(2,1)S(1)} %bitcast.9, f32[1,2048]{1,0:T(1,128)S(1)} %bitcast.11, bf16[2048,256]{1,0:T(8,128)(2,1)S(1)} %collective-permute-done.gate1, bf16[1536,256]{1,0:T(8,128)(2,1)S(1)} %load.1.head0, bf16[2048,256]{1,0:T(8,128)(2,1)} %bitcast.14, ...), custom_call_target="tpu_custom_call" | custom-call | tf_op jit(solution)/shard_map/hidden/pallas_call | solution.py:277
  30.8 0.0 collective-permute-done.2.down1_ref
  30.8 0.5 down.1
  31.4 15.0 %all_to_all.15 = bf16[32,8,1024]{2,1,0:T(8,128)(2,1)S(1)} all-to-all(bf16[32,8,1024]{2,1,0:T(8,128)(2,1)S(1)} %down.1), channel_id=1, replica_groups={{321,320,193,192,289,288,353,352,449,448,65,64,161,160,225,224,257,256,..., dimensions={0} | all-to-all | bytes 1048576 | tf_op jit(solution)/shard_map/all_to_all | solution.py:297
  46.4 0.3 combine.1
  46.6 17.9 %all_to_all.16.parts_ref = bf16[16,16,128]{2,1,0:T(8,128)(2,1)S(1)} all-to-all(bf16[16,16,128]{2,1,0:T(8,128)(2,1)S(1)} %combine.1), channel_id=1, replica_groups={{20,22,24,26,28,30,0,2,4,6,8,10,12,14,16,18},{21,23,25,27,29,31,1,3,5,7..., dimensions={0} | all-to-all | bytes 131072 | tf_op jit(solution)/shard_map/all_to_all | solution.py:306
  64.6 0.7 %total.1 = bf16[32,64]{1,0:T(8,128)(2,1)} custom-call(bf16[16,16,128]{2,1,0:T(8,128)(2,1)S(1)} %all_to_all.16.parts_ref), custom_call_target="tpu_custom_call" | custom-call | tf_op jit(solution)/shard_map/total/pallas_call | solution.py:307
Async XLA Ops:
  0.0 28.5 %collective-permute-start = (bf16[2048,256]{1,0:T(8,128)(2,1)}, bf16[2048,256]{1,0:T(8,128)(2,1)S(1)}, u32[]{:S(2)}, u32[]{:S(2)}) collective-permute-start(bf16[2048,256]{1,0:T(8,128)(2,1)} %bitcast.12), channel_id=1, source_target_pairs={{0,1},{1,0},{2,3},{3,2},{4,5},{5,4},{6,7},{7,6},{8,9},{9,8},{10,11... | collective-permute-start | bytes 3145736 | tf_op jit(solution)/shard_map/ppermute | solution.py:266
  8.7 19.8 %collective-permute-start.1 = (bf16[2048,256]{1,0:T(8,128)(2,1)}, bf16[2048,256]{1,0:T(8,128)(2,1)}, u32[]{:S(2)}, u32[]{:S(2)}) collective-permute-start(bf16[2048,256]{1,0:T(8,128)(2,1)} %bitcast.15), channel_id=1, source_target_pairs={{0,1},{1,0},{2,3},{3,2},{4,5},{5,4},{6,7},{7,6},{8,9},{9,8},{10,11... | collective-permute-start | bytes 3145736 | tf_op jit(solution)/shard_map/ppermute | solution.py:267
  10.7 20.1 %collective-permute-start.2 = (bf16[256,2048]{1,0:T(8,128)(2,1)}, bf16[256,2048]{1,0:T(8,128)(2,1)S(1)}, u32[]{:S(2)}, u32[]{:S(2)}) collective-permute-start(bf16[256,2048]{1,0:T(8,128)(2,1)} %bitcast.17), channel_id=1, source_target_pairs={{0,1},{1,0},{2,3},{3,2},{4,5},{5,4},{6,7},{7,6},{8,9},{9,8},{10,11... | collective-permute-start | bytes 3145736 | tf_op jit(solution)/shard_map/ppermute | solution.py:265
  15.1 13.5 %all-to-all-start = ((bf16[16,8,2048]{2,1,0:T(8,128)(2,1)}), bf16[16,8,2048]{2,1,0:T(8,128)(2,1)S(1)}, u32[]{:S(2)}, u32[]{:S(2)}) async-start(bf16[16,8,2048]{2,1,0:T(8,128)(2,1)} %bitcast.2), calls=%async_computation | async-start | bytes 1048576 | tf_op jit(solution)/shard_map/all_to_all | solution.py:257
  21.7 6.8 %copy-start = (f32[2048]{0:T(1024)S(1)}, f32[2048]{0:T(1024)}, u32[]{:S(2)}) copy-start(f32[2048]{0:T(1024)} %param.9) | copy-start | bytes 24580

commit v7 on v6

--- a/solution.py
+++ b/solution.py
@@ -140,17 +140,16 @@
 def hidden_kernel(
     received_ref,
     gain_ref,
-    gate1,
     head0,
     gate0_hbm,
     up0_hbm,
+    gate1_hbm,
     up1_hbm,
-    down0_hbm,
     hidden_ref,
-    down0_ref,
     rows_ref,
     tail0,
     up0,
+    gate1,
     up1,
     sems,
 ):
@@ -160,21 +159,21 @@
         sems,
         (gate0_hbm.at[pl.ds(cut, tail0.shape[0]), :], tail0),
         (up0_hbm, up0),
+        (gate1_hbm, gate1),
         (up1_hbm, up1),
-        (down0_hbm, down0_ref),
     )
     values = received_ref[...].astype(F32)
     scale = lax.rsqrt(jnp.mean(values * values, axis=-1, keepdims=True) + 1e-06)
     rows_ref[...] = (received_ref[...].astype(F32) * scale * gain_ref[...]).astype(BF16)
-    gate = times(rows_ref[...], gate1)
     own = times(rows_ref[:, :cut], head0)
     copies[0].wait()
     own = own + times(rows_ref[:, cut:], tail0)
     copies[1].wait()
     hidden_ref[:, :units] = hidden_of(own, times(rows_ref[...], up0))
     copies[2].wait()
+    gate = times(rows_ref[...], gate1)
+    copies[3].wait()
     hidden_ref[:, units:] = hidden_of(gate, times(rows_ref[...], up1))
-    copies[3].wait()
 
 
 def down_kernel(hidden_ref, down0_ref, down1_ref, out_ref):
@@ -274,26 +273,27 @@
         compiler_params=params(8),
         name="load",
     )(*in_hbm(w_gate))
-    hidden, down = pl.pallas_call(
+    hidden = pl.pallas_call(
         hidden_kernel,
-        in_specs=[vmem] * 4 + [hbm] * 4,
-        out_shape=(shape((mine, 2 * units), BF16), shape(w_down.shape, BF16)),
+        in_specs=[vmem] * 3 + [hbm] * 4,
+        out_shape=shape((mine, 2 * units), BF16),
         scratch_shapes=[
             pltpu.VMEM((mine, width), BF16),
             pltpu.VMEM((width - cut, units), BF16),
+            pltpu.VMEM(w_gate.shape, BF16),
             pltpu.VMEM(w_up.shape, BF16),
             pltpu.VMEM(w_up.shape, BF16),
             pltpu.SemaphoreType.DMA((4,)),
         ],
         compiler_params=params(8),
         name="hidden",
-    )(received, gain, o_gate, head, *in_hbm(w_gate, w_up, o_up, w_down))
+    )(received, gain, head, *in_hbm(w_gate, w_up, o_gate, o_up))
     outputs = pl.pallas_call(
         down_kernel,
         out_shape=shape((2 * n_ep, each, part), BF16),
         compiler_params=params(8),
         name="down",
-    )(hidden, down, o_down)
+    )(hidden, w_down, o_down)
     back = lax.all_to_all(
         outputs, ("ep", "c"), split_axis=0, concat_axis=0, tiled=True, axis_index_groups=[WAY_BACK]
     ).reshape(slots, part)

time: 65.9 us -> 67.5 us (1.024)
  local copies, waits for them, and re-layouts: 0.01 us -> 1.03 us
    unnamed x2 -> x6, local copies, waits for them, and re-layouts: 0.01 us -> 1.03 us
  transfers between devices with their start and end apart: 4 -> 4, of which waited for: 1 -> 1; matrix products, arithmetic and copies ran while one was open for 0% -> 0% of each run, Pallas kernels for 8% -> 9%
where the time goes in v7:
time: 67.5 us; the launch traced here: 66.8 us
  blocking collectives  32.9 us (49%)
  starting transfers between devices  19.7 us (29%)
  Pallas kernels  7.38 us (11%)
  waiting for transfers between devices  5.64 us (8%)
  local copies, waits for them, and re-layouts  1.03 us (2%)
    all_to_all x1, blocking collectives, shards(): lax.all_to_all(packed, 'z', split_axis=0, concat_axis=0, tiled=True, axis...  17.9 us
    all_to_all x1, blocking collectives, shards(): lax.all_to_all(outputs, ('ep', 'c'), split_axis=0, concat_axis=0, tiled=T...  15 us
    ppermute x1, starting transfers between devices, shards(): o_gate = lax.ppermute(w_gate, 'c', SWAP)  8.74 us
    all_to_all x1, starting transfers between devices, shards(): lax.all_to_all(buffer.reshape(n_ep, each, width), 'ep', split_axis=0, con...  6.68 us
    all_to_all x1, waiting for transfers between devices, shards(): lax.all_to_all(buffer.reshape(n_ep, each, width), 'ep', split_axis=0, con...  5.63 us
    pallas_call x1, Pallas kernels, shards(): pl.pallas_call(hidden_kernel, in_specs=[vmem] * 3 + [hbm] * 4, out_shape=...  2.76 us
    ppermute x1, starting transfers between devices, shards(): o_down = lax.ppermute(w_down, 'c', SWAP)  2.41 us
    pallas_call x1, Pallas kernels, shards(): pl.pallas_call(dispatch_kernel, in_specs=[hbm] * 4, out_shape=(shape((min...  1.96 us
  transfers between devices with their start and end apart: 4, of which 1 were waited for; matrix products, arithmetic and copies ran while one was open for 0% of the time, Pallas kernels for 9%

profile of v7, /device:TPU:1, one launch (start us, length us, event | category | flops | bytes accessed | tf_op | source)
XLA Modules:
  0.0 66.8 jit_solution(15803227855215863757)
XLA Ops:
  0.0 8.7 %collective-permute-start = (bf16[2048,256]{1,0:T(8,128)(2,1)}, bf16[2048,256]{1,0:T(8,128)(2,1)S(1)}, u32[]{:S(2)}, u32[]{:S(2)}) collective-permute-start(bf16[2048,256]{1,0:T(8,128)(2,1)} %bitcast.14), channel_id=1, source_target_pairs={{0,1},{1,0},{2,3},{3,2},{4,5},{5,4},{6,7},{7,6},{8,9},{9,8},{10,11... | collective-permute-start | bytes 3145736 | tf_op jit(solution)/shard_map/ppermute | solution.py:265
  8.7 1.9 %collective-permute-start.1 = (bf16[2048,256]{1,0:T(8,128)(2,1)}, bf16[2048,256]{1,0:T(8,128)(2,1)}, u32[]{:S(2)}, u32[]{:S(2)}) collective-permute-start(bf16[2048,256]{1,0:T(8,128)(2,1)} %bitcast.17), channel_id=1, source_target_pairs={{0,1},{1,0},{2,3},{3,2},{4,5},{5,4},{6,7},{7,6},{8,9},{9,8},{10,11... | collective-permute-start | bytes 3145736 | tf_op jit(solution)/shard_map/ppermute | solution.py:266
  10.7 2.4 %collective-permute-start.2 = (bf16[256,2048]{1,0:T(8,128)(2,1)}, bf16[256,2048]{1,0:T(8,128)(2,1)S(1)}, u32[]{:S(2)}, u32[]{:S(2)}) collective-permute-start(bf16[256,2048]{1,0:T(8,128)(2,1)} %bitcast.11), channel_id=1, source_target_pairs={{0,1},{1,0},{2,3},{3,2},{4,5},{5,4},{6,7},{7,6},{8,9},{9,8},{10,11... | collective-permute-start | bytes 3145736 | tf_op jit(solution)/shard_map/ppermute | solution.py:264
  13.1 2.0 %dispatch.1 = (bf16[128,2048]{1,0:T(8,128)(2,1)}, bf16[64,256]{1,0:T(8,128)(2,1)S(1)}) custom-call(bf16[32,2048]{1,0:T(8,128)(2,1)} %tok_hbm.1, s32[2,32]{1,0:T(2,128)} %bitcast.19, f32[2,32]{1,0:T(2,128)} %bitcast.20, s32[2,256]{1,0:T(2,128)} %constant.2.clone.tables_hbm), custom_call_target="tpu_custom_call" | custom-call | tf_op jit(solution)/shard_map/dispatch/pallas_call | solution.py:239
  15.1 6.7 %all-to-all-start = ((bf16[16,8,2048]{2,1,0:T(8,128)(2,1)}), bf16[16,8,2048]{2,1,0:T(8,128)(2,1)S(1)}, u32[]{:S(2)}, u32[]{:S(2)}) async-start(bf16[16,8,2048]{2,1,0:T(8,128)(2,1)} %bitcast.2), calls=%async_computation | async-start | bytes 1048576 | tf_op jit(solution)/shard_map/all_to_all | solution.py:256
  21.7 0.0 copy-start.1
  21.8 1.1 %load.1.head0 = bf16[1536,256]{1,0:T(8,128)(2,1)S(1)} custom-call(bf16[2048,256]{1,0:T(8,128)(2,1)} %bitcast.15), custom_call_target="tpu_custom_call" | custom-call | tf_op jit(solution)/shard_map/load/pallas_call | solution.py:268
  22.9 5.6 %all-to-all-done = bf16[16,8,2048]{2,1,0:T(8,128)(2,1)S(1)} async-done(((bf16[16,8,2048]{2,1,0:T(8,128)(2,1)}), bf16[16,8,2048]{2,1,0:T(8,128)(2,1)S(1)}, u32[]{:S(2)}, u32[]{:S(2)}) %all-to-all-start) | async-done | bytes 524320 | tf_op jit(solution)/shard_map/all_to_all | solution.py:256
  28.5 0.0 collective-permute-done.gate1_hbm
  28.5 0.0 copy-start.2
  28.5 0.0 collective-permute-done.1.up1_hbm
  28.6 1.0 %copy-done.2 = bf16[2048,256]{1,0:T(8,128)(2,1)} copy-done((bf16[2048,256]{1,0:T(8,128)(2,1)}, bf16[2048,256]{1,0:T(8,128)(2,1)S(1)}, u32[]{:S(2)}) %copy-start.2) | copy-done | bytes 1048600
  29.6 0.0 copy-done.1
  29.6 0.0 copy-start
  29.6 2.8 %hidden.1.hidden_ref = bf16[128,512]{1,0:T(8,128)(2,1)S(1)} custom-call(bf16[128,2048]{1,0:T(8,128)(2,1)S(1)} %bitcast.10, f32[1,2048]{1,0:T(1,128)S(1)} %bitcast.13, bf16[1536,256]{1,0:T(8,128)(2,1)S(1)} %load.1.head0, bf16[2048,256]{1,0:T(8,128)(2,1)} %bitcast.16, bf16[2048,256]{1,0:T(8,128)(2,1)} %bitcast.18, bf16[2048,256]{1,0:T(8,128)(2,1)} %copy-done.2, ...), custom_call_target="tpu_custom_call" | custom-call | tf_op jit(solution)/shard_map/hidden/pallas_call | solution.py:276
  32.3 0.0 collective-permute-done.2.down1_ref
  32.4 0.0 copy-done
  32.4 0.5 down.1
  32.9 15.0 %all_to_all.15 = bf16[32,8,1024]{2,1,0:T(8,128)(2,1)S(1)} all-to-all(bf16[32,8,1024]{2,1,0:T(8,128)(2,1)S(1)} %down.1), channel_id=1, replica_groups={{321,320,193,192,289,288,353,352,449,448,65,64,161,160,225,224,257,256,..., dimensions={0} | all-to-all | bytes 1048576 | tf_op jit(solution)/shard_map/all_to_all | solution.py:297
  47.9 0.3 combine.1
  48.2 17.9 %all_to_all.16.parts_ref = bf16[16,16,128]{2,1,0:T(8,128)(2,1)S(1)} all-to-all(bf16[16,16,128]{2,1,0:T(8,128)(2,1)S(1)} %combine.1), channel_id=1, replica_groups={{20,22,24,26,28,30,0,2,4,6,8,10,12,14,16,18},{21,23,25,27,29,31,1,3,5,7..., dimensions={0} | all-to-all | bytes 131072 | tf_op jit(solution)/shard_map/all_to_all | solution.py:306
  66.1 0.7 %total.1 = bf16[32,64]{1,0:T(8,128)(2,1)} custom-call(bf16[16,16,128]{2,1,0:T(8,128)(2,1)S(1)} %all_to_all.16.parts_ref), custom_call_target="tpu_custom_call" | custom-call | tf_op jit(solution)/shard_map/total/pallas_call | solution.py:307
Async XLA Ops:
  0.0 28.5 %collective-permute-start = (bf16[2048,256]{1,0:T(8,128)(2,1)}, bf16[2048,256]{1,0:T(8,128)(2,1)S(1)}, u32[]{:S(2)}, u32[]{:S(2)}) collective-permute-start(bf16[2048,256]{1,0:T(8,128)(2,1)} %bitcast.14), channel_id=1, source_target_pairs={{0,1},{1,0},{2,3},{3,2},{4,5},{5,4},{6,7},{7,6},{8,9},{9,8},{10,11... | collective-permute-start | bytes 3145736 | tf_op jit(solution)/shard_map/ppermute | solution.py:265
  8.7 19.8 %collective-permute-start.1 = (bf16[2048,256]{1,0:T(8,128)(2,1)}, bf16[2048,256]{1,0:T(8,128)(2,1)}, u32[]{:S(2)}, u32[]{:S(2)}) collective-permute-start(bf16[2048,256]{1,0:T(8,128)(2,1)} %bitcast.17), channel_id=1, source_target_pairs={{0,1},{1,0},{2,3},{3,2},{4,5},{5,4},{6,7},{7,6},{8,9},{9,8},{10,11... | collective-permute-start | bytes 3145736 | tf_op jit(solution)/shard_map/ppermute | solution.py:266
  10.7 21.7 %collective-permute-start.2 = (bf16[256,2048]{1,0:T(8,128)(2,1)}, bf16[256,2048]{1,0:T(8,128)(2,1)S(1)}, u32[]{:S(2)}, u32[]{:S(2)}) collective-permute-start(bf16[256,2048]{1,0:T(8,128)(2,1)} %bitcast.11), channel_id=1, source_target_pairs={{0,1},{1,0},{2,3},{3,2},{4,5},{5,4},{6,7},{7,6},{8,9},{9,8},{10,11... | collective-permute-start | bytes 3145736 | tf_op jit(solution)/shard_map/ppermute | solution.py:264
  15.1 13.5 %all-to-all-start = ((bf16[16,8,2048]{2,1,0:T(8,128)(2,1)}), bf16[16,8,2048]{2,1,0:T(8,128)(2,1)S(1)}, u32[]{:S(2)}, u32[]{:S(2)}) async-start(bf16[16,8,2048]{2,1,0:T(8,128)(2,1)} %bitcast.2), calls=%async_computation | async-start | bytes 1048576 | tf_op jit(solution)/shard_map/all_to_all | solution.py:256
  21.7 7.8 %copy-start.1 = (f32[2048]{0:T(1024)S(1)}, f32[2048]{0:T(1024)}, u32[]{:S(2)}) copy-start(f32[2048]{0:T(1024)} %param.9) | copy-start | bytes 24580
  28.5 1.0 %copy-start.2 = (bf16[2048,256]{1,0:T(8,128)(2,1)}, bf16[2048,256]{1,0:T(8,128)(2,1)S(1)}, u32[]{:S(2)}) copy-start(bf16[2048,256]{1,0:T(8,128)(2,1)S(1)} %collective-permute-done.gate1_hbm) | copy-start | bytes 3145732
  29.6 2.8 %copy-start = (bf16[1,256,2048]{2,1,0:T(8,128)(2,1)S(1)}, bf16[1,256,2048]{2,1,0:T(8,128)(2,1)}, u32[]{:S(2)}) copy-start(bf16[1,256,2048]{2,1,0:T(8,128)(2,1)} %param.14) | copy-start | bytes 3145732
